TPU v7x, 256 devices: a whole 4x4x8 slice. The times are simulated.
256 devices in a mesh: sp: 16 (over y, x), dp: 16 (over z, core).
Axes of the slice: x: 4, y: 4, z: 8, core: 2. Of those that a mesh axis runs over, the one named last changes fastest.
Arguments:
- tokens: bfloat16 [16, 4096, 2048], P('dp', 'sp'), may hold values from -6 to 6
- in_gain: float32 [2048], replicated, may hold values from 0.1 to 1.9
- query_weight: bfloat16 [2048, 2048], P('dp'), may hold values from -1 to 1
- key_weight: bfloat16 [2048, 512], P('dp'), may hold values from -1 to 1
- value_matrix: bfloat16 [2048, 512], P('dp'), may hold values from -0.125 to 0.125
- query_gain: float32 [128], replicated, may hold values from 1 to 6
- key_gain: float32 [128], replicated, may hold values from 1 to 6
- out_weight: bfloat16 [2048, 2048], P('dp'), may hold values from -0.125 to 0.125
- out_gain: float32 [2048], replicated, may hold values from 0.1 to 1.9
Outputs:
- mixed: bfloat16 [16, 4096, 2048], P('dp', 'sp')
All inputs are finite; a program needn't handle non-finite values.
Results may differ from a plain program's by a relative error of at most 0.0055.
The roundings to bfloat16 on the way count: a program that leaves them out, or rounds other values in their place, can miss the bound.
Values may be sent and summed in bfloat16 or wider, within the bound.
A program may use at most 128 MiB of HBM per device.

v0:
```python
import jax
import jax.numpy as jnp
from jax import lax
from jax.sharding import PartitionSpec as P

QUERY_HEAD_COUNT = 16
KEY_VALUE_HEADS = 4
HEAD_WIDTH = 128
GRID_W = 64


EPS = 1e-06
THETA = 10000.0


def in_order(parts, dim):
    parts = jnp.moveaxis(parts, 0, dim)
    shape = parts.shape
    return parts.reshape(*shape[:dim], shape[dim] * shape[dim + 1], *shape[dim + 2 :])


def copy_for_each(x, axis):
    devices = lax.axis_size(axis)
    return lax.all_to_all(jnp.broadcast_to(x[None], (devices, *x.shape)), axis, 0, 0, tiled=True)


def gathered_copies(x, axis, dim):
    return in_order(copy_for_each(x, axis), dim)


def sent_together(arrays, axis, dim, along):
    both = jnp.concatenate(arrays, axis=along)
    filled, at, outs = (gathered_copies(both, axis, dim), 0, [])
    for a in arrays:
        outs.append(lax.slice_in_dim(filled, at, at + a.shape[along], axis=along))
        at += a.shape[along]
    return tuple(outs)


def norm_rows(row_data, gain_vec):
    return (
        row_data * lax.rsqrt(jnp.mean(row_data * row_data, axis=-1, keepdims=True) + EPS) * gain_vec
    )


def rotate(head_data, positions):
    head_size = head_data.shape[-1]
    half_size = head_size // 2
    quarter = head_size // 4
    inverse_freq = THETA ** (-jnp.arange(quarter, dtype=jnp.float32) / quarter)
    row_angle = (positions // GRID_W).astype(jnp.float32)[:, None] * inverse_freq[None, :]
    col_angle = (positions % GRID_W).astype(jnp.float32)[:, None] * inverse_freq[None, :]

    def turn_half(half_part, angle):
        cosine = jnp.cos(angle)[:, None, :]
        sine_val = jnp.sin(angle)[:, None, :]
        first_part = half_part[..., :quarter]
        second_part = half_part[..., quarter:]
        return jnp.concatenate(
            [
                first_part * cosine - second_part * sine_val,
                second_part * cosine + first_part * sine_val,
            ],
            axis=-1,
        )

    return jnp.concatenate(
        [
            turn_half(head_data[..., :half_size], row_angle),
            turn_half(head_data[..., half_size:], col_angle),
        ],
        axis=-1,
    )


def finish(projected, gain_vec, positions):
    row_count = projected.shape[0]
    heads_data = projected.reshape(row_count, -1, HEAD_WIDTH)
    heads_data = rotate(norm_rows(heads_data, gain_vec), positions)
    return heads_data.reshape(row_count, -1).astype(jnp.bfloat16)


def attend(local_q, local_k, local_v, heads_local, key_value_slice):
    length = local_q.shape[0]
    group_local = heads_local // key_value_slice
    rows_per_block = min(512, length)
    query_block_list = local_q.reshape(
        length // rows_per_block, rows_per_block, key_value_slice, group_local, HEAD_WIDTH
    )
    key_heads = local_k.reshape(length, key_value_slice, HEAD_WIDTH)
    value_heads = local_v.reshape(length, key_value_slice, HEAD_WIDTH)

    def one_block(query_block):
        scores = jnp.einsum(
            "qegd,ked->egqk", query_block, key_heads, preferred_element_type=jnp.float32
        ) * HEAD_WIDTH ** (-0.5)
        shifted = scores - jnp.max(scores, axis=-1, keepdims=True)
        raised = jnp.exp(shifted)
        weights = (raised / jnp.sum(raised, axis=-1, keepdims=True)).astype(jnp.bfloat16)
        attended = jnp.einsum(
            "egqk,ked->qegd", weights, value_heads, preferred_element_type=jnp.float32
        )
        return attended.astype(jnp.bfloat16)

    return lax.map(one_block, query_block_list).reshape(length, heads_local * HEAD_WIDTH)


def on_device(
    tokens,
    in_gain,
    query_weight,
    key_weight,
    value_matrix,
    query_gain,
    key_gain,
    out_weight,
    out_gain,
):
    sequence = tokens[0]
    repeat_heads = lax.axis_size("sp")
    sp_rank = lax.axis_index("sp")
    heads_local = QUERY_HEAD_COUNT // repeat_heads
    key_value_slice = max(1, KEY_VALUE_HEADS // repeat_heads)
    queries_per_group = QUERY_HEAD_COUNT // KEY_VALUE_HEADS
    first_kv = sp_rank * heads_local // queries_per_group
    normed = norm_rows(sequence.astype(jnp.float32), in_gain).astype(jnp.bfloat16)
    q_cols = lax.dynamic_slice_in_dim(
        query_weight, sp_rank * heads_local * HEAD_WIDTH, heads_local * HEAD_WIDTH, 1
    )
    k_cols = lax.dynamic_slice_in_dim(
        key_weight, first_kv * HEAD_WIDTH, key_value_slice * HEAD_WIDTH, 1
    )
    v_cols = lax.dynamic_slice_in_dim(
        value_matrix, first_kv * HEAD_WIDTH, key_value_slice * HEAD_WIDTH, 1
    )
    full_q, full_k, full_v = sent_together((q_cols, k_cols, v_cols), "dp", 0, 1)
    joined = jnp.concatenate([full_q, full_k, full_v], axis=1)
    query_end = heads_local * HEAD_WIDTH
    key_end = query_end + key_value_slice * HEAD_WIDTH
    shard_rows = lax.all_gather(normed, "sp", axis=0, tiled=True)
    row_count = shard_rows.shape[0]
    blended = jnp.dot(shard_rows, joined, preferred_element_type=jnp.float32)
    positions = jnp.arange(row_count, dtype=jnp.int32)
    part_q = finish(blended[:, :query_end], query_gain, positions)
    part_k = finish(blended[:, query_end:key_end], key_gain, positions)
    part_v = blended[:, key_end:].astype(jnp.bfloat16)
    merged = jnp.concatenate([part_q, part_k, part_v], axis=1)
    local_q = merged[:, :query_end]
    local_k = merged[:, query_end:key_end]
    local_v = merged[:, key_end:]
    attended = attend(local_q, local_k, local_v, heads_local, key_value_slice)
    returned = lax.all_to_all(attended, "sp", split_axis=0, concat_axis=1, tiled=True)
    projected = jnp.dot(
        returned,
        lax.all_gather(out_weight, "dp", axis=0, tiled=True),
        preferred_element_type=jnp.float32,
    )
    result = norm_rows(projected, out_gain).astype(jnp.bfloat16)
    return result[None]


def solution(mesh):
    placed = (
        P("dp", "sp", None),
        P(),
        P("dp", None),
        P("dp", None),
        P("dp", None),
        P(),
        P(),
        P("dp", None),
        P(),
    )
    return jax.shard_map(
        on_device, mesh=mesh, in_specs=placed, out_specs=P("dp", "sp", None), check_vma=False
    )
```

profile of v0, /device:TPU:1, one launch (start us, length us, event | category | flops | bytes accessed | tf_op | source)
XLA Modules:
  0.0 247.1 jit_solution(5400596723069896770)
XLA Ops:
  6.5 1.6 fusion.21
  8.1 2.5 %fusion.23 = bf16[256,2048]{1,0:T(8,128)(2,1)} fusion(bf16[1,256,2048]{2,1,0:T(8,128)(2,1)} %param.11, f32[2048]{0:T(1024)} %param.12, f32[256]{0:T(256)S(1)} %add_rsqrt_fusion.3), kind=kLoop, calls=%fused_computation.22 | loop fusion | flops 2097152 | bytes 2106368 | tf_op jit(solution)/shard_map/convert_element_type | solution.py:126
  13.0 10.0 %all-to-all-start = ((bf16[16,128,384]{2,1,0:T(8,128)(2,1)}), bf16[16,128,384]{2,1,0:T(8,128)(2,1)S(1)}, u32[]{:S(2)}, u32[]{:S(2)}) async-start(bf16[16,128,384]{2,1,0:T(8,128)(2,1)} %broadcast_in_dim.10), calls=%async_computation | async-start | bytes 3145728 | tf_op jit(solution)/shard_map/all_to_all | solution.py:24
  23.7 37.7 %all-to-all-done = bf16[16,128,384]{2,1,0:T(8,128)(2,1)S(1)} async-done(((bf16[16,128,384]{2,1,0:T(8,128)(2,1)}), bf16[16,128,384]{2,1,0:T(8,128)(2,1)S(1)}, u32[]{:S(2)}, u32[]{:S(2)}) %all-to-all-start) | async-done | bytes 1572896 | tf_op jit(solution)/shard_map/all_to_all | solution.py:24
  61.5 69.2 %all-gather.3.cloned.1.call-done = bf16[4096,2048]{1,0:T(8,128)(2,1)} async-done(((bf16[256,2048]{1,0:T(8,128)(2,1)}), bf16[4096,2048]{1,0:T(8,128)(2,1)}) %all-gather.3.cloned.1.call-update) | async-done | bytes 16777232 | tf_op jit(solution)/shard_map/all_gather | solution.py:140
  130.7 10.7 %fusion.67 = f32[4096,384]{0,1:T(8,128)S(1)} fusion(bf16[4096,2048]{1,0:T(8,128)(2,1)} %all-gather.3.cloned.1.call-done, bf16[2048,384]{1,0:T(8,128)(2,1)S(1)} %bitcast.91), kind=kOutput, calls=%fused_computation.92 | convolution fusion | flops 6442450944 | bytes 24641536 | tf_op jit(solution)/shard_map/dot_general | solution.py:142
  143.0 5.1 %fusion.43 = (bf16[4096,1,32]{0,2,1:T(8,128)(2,1)S(1)}, bf16[4096,1,32]{0,2,1:T(8,128)(2,1)S(1)}, bf16[4096,1,32]{0,2,1:T(8,128)(2,1)S(1)}, bf16[4096,1,32]{0,2,...) fusion(f32[4096,1,128]{0,2,1:T(8,128)S(1)} %get-tuple-element.6, ...), kind=kLoop, calls=%fused_computation.55 | loop fusion | flops 4456448 | bytes 6324352 | tf_op jit(solution)/shard_map/convert.7
  149.2 1.6 copy.17
  150.8 2.0 pad_maximum_fusion
  152.8 2.2 copy.20
  156.4 55.1 %while.10 = (s32[]{:T(128)}, bf16[8,512,1,1,128]{4,1,3,2,0:T(8,128)(2,1)}, bf16[8,512,1,1,128]{4,1,3,2,0:T(8,128)(2,1)}, bf16[4096,1,128]{2,0,1:T(8,128)(2,1)S(1)}, bf16[4096,1,128]{2,0,1:T(8,128)(2,1)}, /*index=5*/s32[]{:T(128)}) while((s32[]{:T(128)}, bf16[8,512,1,1,128]{4,1,3,2,0:T(8,128)(2,1)}, bf16[8,512,1,1,128]{4,1,3,2,0:T(8,128)(2,1)}, ...), condition=%wide.region_6.7_spmd, body=%wide.region_3.6_spmd.sunk | while | flops 1092680704 | bytes 31730784 | solution.py:105
  156.4 2.2 multiply_reduce_fusion.5
  158.6 1.5 fusion.78
  160.1 3.1 %fusion.79 = bf16[8,512,1,1,128]{4,1,3,2,0:T(8,128)(2,1)} fusion(bf16[8,512,1,1,128]{4,1,3,2,0:T(8,128)(2,1)} %get-tuple-element.128, s32[]{:T(128)} %get-tuple-element.127, f32[512]{0:T(512)S(1)} %fusion.78, f32[512]{0:T(512)S(1)} %get-tuple-element.120, f32[512,4096]{1,0:T(8,128)S(1)} %get-tuple-element.119, bf16[4096,1,128]{2,0,1:T(8,128)(2,1)S(1)} %copy-done.1), kind=kOutput, calls=%fused_computation.10.clone.1 | convolution fusion | flops 545325056 | bytes 9572864 | tf_op jit(solution)/shard_map/while/body/eval_jaxpr/egqk,ked->qegd/dot_general | solution.py:100
  163.3 2.2 multiply_reduce_fusion.5
  165.5 1.5 fusion.78
  167.0 3.1 %fusion.79 = bf16[8,512,1,1,128]{4,1,3,2,0:T(8,128)(2,1)} fusion(bf16[8,512,1,1,128]{4,1,3,2,0:T(8,128)(2,1)} %get-tuple-element.128, s32[]{:T(128)} %get-tuple-element.127, f32[512]{0:T(512)S(1)} %fusion.78, f32[512]{0:T(512)S(1)} %get-tuple-element.120, f32[512,4096]{1,0:T(8,128)S(1)} %get-tuple-element.119, bf16[4096,1,128]{2,0,1:T(8,128)(2,1)S(1)} %copy-done.1), kind=kOutput, calls=%fused_computation.10.clone.1 | convolution fusion | flops 545325056 | bytes 9572864 | tf_op jit(solution)/shard_map/while/body/eval_jaxpr/egqk,ked->qegd/dot_general | solution.py:100
  170.2 2.2 multiply_reduce_fusion.5
  172.4 1.5 fusion.78
  173.9 3.1 %fusion.79 = bf16[8,512,1,1,128]{4,1,3,2,0:T(8,128)(2,1)} fusion(bf16[8,512,1,1,128]{4,1,3,2,0:T(8,128)(2,1)} %get-tuple-element.128, s32[]{:T(128)} %get-tuple-element.127, f32[512]{0:T(512)S(1)} %fusion.78, f32[512]{0:T(512)S(1)} %get-tuple-element.120, f32[512,4096]{1,0:T(8,128)S(1)} %get-tuple-element.119, bf16[4096,1,128]{2,0,1:T(8,128)(2,1)S(1)} %copy-done.1), kind=kOutput, calls=%fused_computation.10.clone.1 | convolution fusion | flops 545325056 | bytes 9572864 | tf_op jit(solution)/shard_map/while/body/eval_jaxpr/egqk,ked->qegd/dot_general | solution.py:100
  177.1 2.3 multiply_reduce_fusion.5
  180.8 3.1 %fusion.79 = bf16[8,512,1,1,128]{4,1,3,2,0:T(8,128)(2,1)} fusion(bf16[8,512,1,1,128]{4,1,3,2,0:T(8,128)(2,1)} %get-tuple-element.128, s32[]{:T(128)} %get-tuple-element.127, f32[512]{0:T(512)S(1)} %fusion.78, f32[512]{0:T(512)S(1)} %get-tuple-element.120, f32[512,4096]{1,0:T(8,128)S(1)} %get-tuple-element.119, bf16[4096,1,128]{2,0,1:T(8,128)(2,1)S(1)} %copy-done.1), kind=kOutput, calls=%fused_computation.10.clone.1 | convolution fusion | flops 545325056 | bytes 9572864 | tf_op jit(solution)/shard_map/while/body/eval_jaxpr/egqk,ked->qegd/dot_general | solution.py:100
  184.0 2.2 multiply_reduce_fusion.5
  187.7 3.1 %fusion.79 = bf16[8,512,1,1,128]{4,1,3,2,0:T(8,128)(2,1)} fusion(bf16[8,512,1,1,128]{4,1,3,2,0:T(8,128)(2,1)} %get-tuple-element.128, s32[]{:T(128)} %get-tuple-element.127, f32[512]{0:T(512)S(1)} %fusion.78, f32[512]{0:T(512)S(1)} %get-tuple-element.120, f32[512,4096]{1,0:T(8,128)S(1)} %get-tuple-element.119, bf16[4096,1,128]{2,0,1:T(8,128)(2,1)S(1)} %copy-done.1), kind=kOutput, calls=%fused_computation.10.clone.1 | convolution fusion | flops 545325056 | bytes 9572864 | tf_op jit(solution)/shard_map/while/body/eval_jaxpr/egqk,ked->qegd/dot_general | solution.py:100
  190.9 2.2 multiply_reduce_fusion.5
  194.6 3.1 %fusion.79 = bf16[8,512,1,1,128]{4,1,3,2,0:T(8,128)(2,1)} fusion(bf16[8,512,1,1,128]{4,1,3,2,0:T(8,128)(2,1)} %get-tuple-element.128, s32[]{:T(128)} %get-tuple-element.127, f32[512]{0:T(512)S(1)} %fusion.78, f32[512]{0:T(512)S(1)} %get-tuple-element.120, f32[512,4096]{1,0:T(8,128)S(1)} %get-tuple-element.119, bf16[4096,1,128]{2,0,1:T(8,128)(2,1)S(1)} %copy-done.1), kind=kOutput, calls=%fused_computation.10.clone.1 | convolution fusion | flops 545325056 | bytes 9572864 | tf_op jit(solution)/shard_map/while/body/eval_jaxpr/egqk,ked->qegd/dot_general | solution.py:100
  197.8 2.2 multiply_reduce_fusion.5
  201.5 3.1 %fusion.79 = bf16[8,512,1,1,128]{4,1,3,2,0:T(8,128)(2,1)} fusion(bf16[8,512,1,1,128]{4,1,3,2,0:T(8,128)(2,1)} %get-tuple-element.128, s32[]{:T(128)} %get-tuple-element.127, f32[512]{0:T(512)S(1)} %fusion.78, f32[512]{0:T(512)S(1)} %get-tuple-element.120, f32[512,4096]{1,0:T(8,128)S(1)} %get-tuple-element.119, bf16[4096,1,128]{2,0,1:T(8,128)(2,1)S(1)} %copy-done.1), kind=kOutput, calls=%fused_computation.10.clone.1 | convolution fusion | flops 545325056 | bytes 9572864 | tf_op jit(solution)/shard_map/while/body/eval_jaxpr/egqk,ked->qegd/dot_general | solution.py:100
  204.6 2.2 multiply_reduce_fusion.5
  208.4 3.1 %fusion.79 = bf16[8,512,1,1,128]{4,1,3,2,0:T(8,128)(2,1)} fusion(bf16[8,512,1,1,128]{4,1,3,2,0:T(8,128)(2,1)} %get-tuple-element.128, s32[]{:T(128)} %get-tuple-element.127, f32[512]{0:T(512)S(1)} %fusion.78, f32[512]{0:T(512)S(1)} %get-tuple-element.120, f32[512,4096]{1,0:T(8,128)S(1)} %get-tuple-element.119, bf16[4096,1,128]{2,0,1:T(8,128)(2,1)S(1)} %copy-done.1), kind=kOutput, calls=%fused_computation.10.clone.1 | convolution fusion | flops 545325056 | bytes 9572864 | tf_op jit(solution)/shard_map/while/body/eval_jaxpr/egqk,ked->qegd/dot_general | solution.py:100
  211.5 21.1 %all_to_all.24 = bf16[16,256,128]{2,1,0:T(8,128)(2,1)S(1)} all-to-all(bf16[16,256,128]{2,1,0:T(8,128)(2,1)} %bitcast.92), channel_id=1, replica_groups=mesh['sp'=16,'dp'=16] {'sp'}, dimensions={0} | all-to-all | bytes 2097152 | tf_op jit(solution)/shard_map/all_to_all | solution.py:152
  233.2 5.8 %multiply_reduce_fusion.1 = (f32[256]{0:T(256)S(1)}, f32[256,2048]{1,0:T(8,128)S(1)}) fusion(bf16[256,2048]{0,1:T(8,128)(2,1)S(1)} %bitcast.88, bf16[2048,2048]{1,0:T(8,128)(2,1)} %all-gather.5.cloned.1.call-done), kind=kOutput, calls=%fused_computation.25 | convolution fusion | flops 2148531968 | bytes 11535360 | tf_op jit(solution)/shard_map/dot_general | solution.py:153
  (52 shorter events, 16.3 us)
Async XLA Ops:
  6.5 4.2 %copy-start = (bf16[128,2048]{1,0:T(8,128)(2,1)S(1)}, bf16[128,2048]{1,0:T(8,128)(2,1)}, u32[]{:S(2)}) copy-start(bf16[128,2048]{1,0:T(8,128)(2,1)} %param.13) | copy-start | bytes 1572868
  6.5 124.1 %all-gather.3.cloned.1.call-start = ((), (), s32[]{:S(2)}) async-start(), calls=%async_computation.2 | async-start | bytes 17825792 | tf_op jit(solution)/shard_map/all_gather | solution.py:140
  13.0 48.5 %all-to-all-start = ((bf16[16,128,384]{2,1,0:T(8,128)(2,1)}), bf16[16,128,384]{2,1,0:T(8,128)(2,1)S(1)}, u32[]{:S(2)}, u32[]{:S(2)}) async-start(bf16[16,128,384]{2,1,0:T(8,128)(2,1)} %broadcast_in_dim.10), calls=%async_computation | async-start | bytes 3145728 | tf_op jit(solution)/shard_map/all_to_all | solution.py:24
  22.9 210.2 %all-gather.5.cloned.1.call-start = ((), (), s32[]{:S(2)}) async-start(), calls=%async_computation.3 | async-start | bytes 8912896 | tf_op jit(solution)/shard_map/all_gather | solution.py:155
  141.7 0.7 copy-start.3
  141.8 0.7 copy-start.4
  158.6 1.5 copy-start.1
  165.5 1.5 copy-start.1
  172.4 1.5 copy-start.1
  179.3 1.5 copy-start.1
  186.2 1.5 copy-start.1
  193.1 1.5 copy-start.1
  200.0 1.5 copy-start.1
  206.9 1.5 copy-start.1
  233.2 5.8 %copy-start.2 = (f32[2048]{0:T(1024)S(1)}, f32[2048]{0:T(1024)}, u32[]{:S(2)}) copy-start(f32[2048]{0:T(1024)} %param.19) | copy-start | bytes 24580
Sparse Core Ops, SparseCore 0:
  10.8 119.8 all-gather.2
  132.5 56.1 all-gather.4
where the time goes:
time: 248 us; the launch traced here: 247 us
  waiting for transfers between devices  108 us (44%)
  matrix products  59.5 us (24%)
  other arithmetic  26.5 us (11%)
  blocking collectives  21.1 us (9%)
  between operations  13.6 us (5%)
  starting transfers between devices  10 us (4%)
  local copies, waits for them, and re-layouts  8.59 us (3%)
    all_gather x1, waiting for transfers between devices, on_device(): shard_rows = lax.all_gather(normed, 'sp', axis=0, tiled=True)  69.2 us
    all_to_all x1, waiting for transfers between devices, copy_for_each(): lax.all_to_all(jnp.broadcast_to(x[None], (devices, *x.shape)), axis, 0, 0...  37.7 us
    dot_general x8, matrix products, one_block(): jnp.einsum('egqk,ked->qegd', weights, value_heads, preferred_element_type...  25.1 us
    all_to_all x1, blocking collectives, on_device(): lax.all_to_all(attended, 'sp', split_axis=0, concat_axis=1, tiled=True)  21.1 us
    dot_general x8, matrix products, one_block(): jnp.einsum('qegd,ked->egqk', query_block, key_heads, preferred_element_ty...  17.9 us
    reduce_sum x8, other arithmetic, one_block(): jnp.sum(raised, axis=-1, keepdims=True)  12 us
    dot_general x1, matrix products, on_device(): blended = jnp.dot(shard_rows, joined, preferred_element_type=jnp.float32)  10.7 us
    all_to_all x1, starting transfers between devices, copy_for_each(): lax.all_to_all(jnp.broadcast_to(x[None], (devices, *x.shape)), axis, 0, 0...  9.97 us
  transfers between devices with their start and end apart: 3, of which 2 were waited for; matrix products, arithmetic and copies ran while one was open for 34% of the time, Pallas kernels for 0%

commit v1 on v0

v1 whole, which is shorter than its diff:
```python
import jax
import jax.numpy as jnp
from jax import lax
from jax.experimental import pallas as pl
from jax.experimental.pallas import tpu as pltpu
from jax.sharding import PartitionSpec as P

MESH = pl.DeviceIdType.MESH
F32 = jnp.float32
BF16 = jnp.bfloat16

EPS = 1e-06
THETA = 10000.0
GRID_W = 64
HEAD = 128
WIDTH = 2048
ROWS = 256
GROUP = 4
KEYS = GROUP * ROWS
Z = 8
SHARD = WIDTH // (2 * Z)
CUT = 768
HALF = ROWS // 2
BQ = 512
TILES = KEYS * GROUP // BQ
ONES = 16
LOG2E = 1.4426950408889634


def span(index, size):
    return pl.ds(pl.multiple_of(index * size, size), size)


def kernel(
    tokens,
    in_gain,
    wq,
    wk,
    wv,
    q_gain,
    k_gain,
    wo,
    out_gain,
    out,
    raw,
    normed,
    weights,
    out_weights,
    cosines,
    sines,
    qt,
    kbuf,
    vbuf,
    s0,
    s1,
    top0,
    top1,
    row_max,
    acc,
    attended,
    returned,
    projected,
    ag_send,
    ag_recv,
    zw_send,
    zw_recv,
    cw_send,
    cw_recv,
    zo_send,
    zo_recv,
    co_send,
    co_recv,
    kv_send,
    kv_recv,
    ret_send,
    ret_recv,
):
    sp = lax.axis_index("sp")
    dp = lax.axis_index("dp")
    y, x = sp // 4, sp % 4
    z, core = dp // 2, dp % 2
    at = (1 - core) * y + core * x
    group = (y + x) % 4

    def member(step):
        to = (at + step) % 4
        return (1 - core) * (to * 4 + x) + core * (y * 4 + to)

    def diagonal(step):
        return ((y + 4 - step) % 4) * 4 + (x + step) % 4

    up = {"dp": ((z + 1) % Z) * 2 + core}
    down = {"dp": ((z + Z - 1) % Z) * 2 + core}
    twin = {"dp": z * 2 + 1 - core}
    peers = [{"sp": member(1)}, {"sp": member(3)}, {"sp": member(2)}]
    peers += [{"sp": diagonal(1)}, {"sp": diagonal(3)}, up, down, twin]

    barrier = pltpu.get_barrier_semaphore()
    for peer in peers:
        pl.semaphore_signal(barrier, inc=1, device_id=peer, device_id_type=MESH)
    pl.semaphore_wait(barrier, len(peers))

    sent = []

    def send(src, dst, send_sem, recv_sem, to):
        copy = pltpu.make_async_remote_copy(
            src_ref=src,
            dst_ref=dst,
            send_sem=send_sem,
            recv_sem=recv_sem,
            device_id=to,
            device_id_type=MESH,
        )
        copy.start()
        return copy

    def arrival(ref, sem):
        pltpu.make_async_copy(ref, ref, sem).wait()

    low, high = pl.ds(0, HALF), pl.ds(HALF, HALF)
    nxt, prv = {"sp": member(1)}, {"sp": member(3)}

    def token_send(src, slot, part, index, to):
        sent.append(
            send(src, raw.at[slot - 1, part], ag_send.at[index], ag_recv.at[index], to)
        )

    token_send(tokens.at[0, low], 3, low, 0, nxt)
    token_send(tokens.at[0, high], 1, high, 1, prv)
    token_send(tokens.at[0, high], 3, high, 2, nxt)
    token_send(tokens.at[0, low], 1, low, 3, prv)

    chunks = (pl.ds(0, SHARD // 2), pl.ds(SHARD // 2, SHARD // 2))
    q_cols = span(group, 512)
    kv_cols = span(group, HEAD)

    def first_weights(part, send_sem, recv_sem, to):
        mine = weights.at[dp, part]
        for src, cols in (
            (wq.at[part, q_cols], pl.ds(0, 512)),
            (wk.at[part, kv_cols], pl.ds(512, HEAD)),
            (wv.at[part, kv_cols], pl.ds(640, HEAD)),
        ):
            send(src, mine.at[:, cols], send_sem, recv_sem, to)
        sent.append(
            pltpu.make_async_remote_copy(
                src_ref=mine,
                dst_ref=mine,
                send_sem=send_sem,
                recv_sem=recv_sem,
                device_id=to,
                device_id_type=MESH,
            )
        )

    for i in (0, 1):
        first_weights(chunks[i], zw_send.at[0, 0, i], zw_recv.at[0, 0, i], up)
        first_weights(chunks[i], zw_send.at[1, 0, i], zw_recv.at[1, 0, i], down)
    for i in (0, 1):
        first_weights(chunks[i], cw_send.at[0, i], cw_recv.at[0, i], twin)

    weights[dp, :, 0:512] = wq[:, q_cols]
    weights[dp, :, 512:640] = wk[:, kv_cols]
    weights[dp, :, 640:768] = wv[:, kv_cols]
    out_weights[dp] = wo[...]

    def ring_event(buf, zs, zr, cs, cr, way, step, i):
        source = (((z + Z - step) % Z) if way == 0 else ((z + step) % Z)) * 2 + core
        part = buf.at[source, chunks[i]]
        arrival(part, zr.at[way, step - 1, i])
        if step < 3 or (step == 3 and i == way):
            sent.append(
                send(part, part, zs.at[way, step, i], zr.at[way, step, i], (up, down)[way])
            )
        slot = step if way == 0 else Z - step
        sent.append(send(part, part, cs.at[slot, i], cr.at[slot, i], twin))

    def weight_event(way, step, i):
        ring_event(weights, zw_send, zw_recv, cw_send, cw_recv, way, step, i)

    def out_event(way, step, i):
        ring_event(out_weights, zo_send, zo_recv, co_send, co_recv, way, step, i)

    gain_in = in_gain[...]

    def normalize(src, slot):
        def rows(i, c):
            part = pl.ds(pl.multiple_of(i * 32, 32), 32)
            v = src[part, :].astype(F32)
            ms = jnp.mean(v * v, axis=-1, keepdims=True)
            normed[slot, part, :] = (v * lax.rsqrt(ms + EPS) * gain_in).astype(BF16)
            return c

        lax.fori_loop(0, ROWS // 32, rows, 0)

    def angles(slot, c):
        row = lax.broadcasted_iota(jnp.int32, (ROWS, HEAD), 0)
        lane = lax.broadcasted_iota(jnp.int32, (ROWS, HEAD), 1)
        power = (lane % 32).astype(F32) * (1.0 / 32.0)
        freq = jnp.exp(power * (-9.210340371976184))
        grid_row = member(slot) * (ROWS // GRID_W) + row // GRID_W
        place = jnp.where(lane < 64, grid_row, row % GRID_W).astype(F32)
        angle = place * freq
        cosines[slot] = jnp.cos(angle)
        sine = jnp.sin(angle)
        sines[slot] = jnp.where(lane % 64 < 32, -sine, sine)
        return c

    for i in (0, 1):
        weight_event(0, 1, i)
        weight_event(1, 1, i)
    normalize(tokens.at[0], 0)
    arrival(raw.at[2, low], ag_recv.at[0])
    token_send(raw.at[2, low], 2, low, 4, nxt)
    arrival(raw.at[0, high], ag_recv.at[1])
    token_send(raw.at[0, high], 2, high, 5, prv)
    for i in (0, 1):
        weight_event(0, 2, i)
        weight_event(1, 2, i)
    lax.fori_loop(0, GROUP, angles, 0)
    for i in (0, 1):
        weight_event(0, 3, i)
        weight_event(1, 3, i)
    arrival(raw.at[2, high], ag_recv.at[2])
    arrival(raw.at[0, low], ag_recv.at[3])
    normalize(raw.at[2], 3)
    normalize(raw.at[0], 1)
    weight_event(0, 4, 0)
    weight_event(1, 4, 1)

    for i in (0, 1):
        for way, to in ((0, up), (1, down)):
            part = out_weights.at[dp, chunks[i]]
            sent.append(
                send(wo.at[chunks[i]], part, zo_send.at[way, 0, i], zo_recv.at[way, 0, i], to)
            )
    for i in (0, 1):
        part = out_weights.at[dp, chunks[i]]
        sent.append(send(wo.at[chunks[i]], part, co_send.at[0, i], co_recv.at[0, i], twin))

    def twin_arrivals(buf, cr):
        for slot in range(Z):
            source = ((z + Z - slot) % Z) * 2 + 1 - core
            for i in (0, 1):
                arrival(buf.at[source, chunks[i]], cr.at[slot, i])

    twin_arrivals(weights, cw_recv)
    arrival(raw.at[1, low], ag_recv.at[4])
    arrival(raw.at[1, high], ag_recv.at[5])
    normalize(raw.at[1], 2)

    gain_q, gain_k = q_gain[...], k_gain[...]

    def project(slot, c):
        cut = weights[...].reshape(WIDTH, CUT)
        values = jnp.dot(normed[slot], cut, preferred_element_type=F32)
        cosine, sine = cosines[slot], sines[slot]
        lane = lax.broadcasted_iota(jnp.int32, (ROWS, HEAD), 1)
        first = lane % 64 < 32

        def finish(v, gain):
            ms = jnp.mean(v * v, axis=-1, keepdims=True)
            v = v * lax.rsqrt(ms + EPS) * gain
            other = jnp.where(first, pltpu.roll(v, HEAD - 32, 1), pltpu.roll(v, 32, 1))
            return v * cosine + other * sine

        for h in range(4):
            q = finish(values[:, h * HEAD : (h + 1) * HEAD], gain_q)
            q = q.astype(BF16).astype(F32).T * (HEAD**-0.5 * LOG2E)
            coarse = q.astype(BF16)
            fine = (q - coarse.astype(F32)).astype(BF16)
            cols = pl.ds(pl.multiple_of(slot * KEYS + h * ROWS, ROWS), ROWS)
            qt[0:HEAD, cols] = coarse
            qt[HEAD : 2 * HEAD, cols] = fine
        rows = span(slot, ROWS)
        kbuf[0, rows, :] = finish(values[:, 512:640], gain_k).astype(BF16)
        vbuf[0, 0:HEAD, rows] = values[:, 640:768].T.astype(BF16)
        return c

    lax.fori_loop(0, GROUP, project, 0)

    def kv_send_to(src, slot, what, index, to):
        buf = kbuf if what == 0 else vbuf
        whole = pl.ds(0, KEYS) if what == 0 else pl.ds(0, HEAD)
        sent.append(
            send(
                buf.at[src, whole],
                buf.at[slot, whole],
                kv_send.at[index],
                kv_recv.at[index],
                {"sp": diagonal(to)},
            )
        )

    kv_send_to(0, 3, 0, 0, 1)
    kv_send_to(0, 1, 1, 1, 3)
    kv_send_to(0, 3, 1, 2, 1)
    kv_send_to(0, 1, 0, 3, 3)

    ones = jnp.ones((ONES, KEYS), BF16)
    for d in range(GROUP):
        vbuf[d, HEAD : HEAD + ONES, :] = ones
    row_max[...] = jnp.full_like(row_max, -1e30)
    acc[...] = jnp.zeros_like(acc)

    def attend(block, nt, sn, topn, ct, sc, topc):
        size = 256
        if sc is not None:
            cols = span(ct, BQ)
            old = row_max[:, cols]
            new = jnp.maximum(old, jnp.max(topc[...], axis=0, keepdims=True))
            row_max[:, cols] = new
            decay = jnp.exp2(old - new)
        top, total = None, None
        for c in range(KEYS // size):
            part = pl.ds(c * size, size)
            if sn is not None:
                k = kbuf[block, part, :]
                s = jnp.dot(
                    jnp.concatenate([k, k], axis=1),
                    qt[:, span(nt, BQ)],
                    preferred_element_type=F32,
                )
                sn[part, :] = s
                most = jnp.max(s.reshape(size // 8, 8, BQ), axis=0)
                top = most if top is None else jnp.maximum(top, most)
            if sc is not None:
                p = jnp.exp2(sc[part, :] - new).astype(BF16)
                d = jnp.dot(vbuf[block, :, part], p, preferred_element_type=F32)
                total = d if total is None else total + d
        if sn is not None:
            topn[...] = top
        if sc is not None:
            acc[:, cols] = acc[:, cols] * decay + total

    def attend_block(block):
        attend(block, 0, s0, top0, None, None, None)

        def pair(i, c):
            t = i * 2
            attend(block, t + 1, s1, top1, t, s0, top0)
            attend(block, (t + 2) % TILES, s0, top0, t + 1, s1, top1)
            return c

        lax.fori_loop(0, TILES // 2, pair, 0)

    attend_block(0)
    for i in (0, 1):
        out_event(0, 1, i)
        out_event(1, 1, i)
    k_all, v_all = pl.ds(0, KEYS), pl.ds(0, HEAD)
    arrival(kbuf.at[3, k_all], kv_recv.at[0])
    kv_send_to(3, 2, 0, 4, 1)
    arrival(vbuf.at[1, v_all], kv_recv.at[1])
    kv_send_to(1, 2, 1, 5, 3)
    arrival(vbuf.at[3, v_all], kv_recv.at[2])
    arrival(kbuf.at[1, k_all], kv_recv.at[3])
    attend_block(3)
    attend_block(1)
    for i in (0, 1):
        out_event(0, 2, i)
        out_event(1, 2, i)
    arrival(kbuf.at[2, k_all], kv_recv.at[4])
    arrival(vbuf.at[2, v_all], kv_recv.at[5])
    attend_block(2)

    def hand_back(slot):
        for h in range(4):
            cols = pl.ds(slot * KEYS + h * ROWS, ROWS)
            scaled = acc[0:HEAD, cols] / acc[HEAD : HEAD + 1, cols]
            attended[slot, :, h * HEAD : (h + 1) * HEAD] = scaled.T.astype(BF16)

    for slot in (2, 1, 3):
        hand_back(slot)
        sent.append(
            send(
                attended.at[slot],
                returned.at[group],
                ret_send.at[slot - 1],
                ret_recv.at[slot - 1],
                {"sp": member(slot)},
            )
        )
    hand_back(0)
    returned[group] = attended[0]
    for i in (0, 1):
        out_event(0, 3, i)
        out_event(1, 3, i)
    out_event(0, 4, 0)
    out_event(1, 4, 1)
    for slot in (1, 2, 3):
        arrival(returned.at[(group + 4 - slot) % 4], ret_recv.at[slot - 1])
    twin_arrivals(out_weights, co_recv)

    squares = jnp.zeros((ROWS, 1), F32)
    for n in range(4):
        cols = slice(n * 512, (n + 1) * 512)
        total = None
        for g in range(4):
            w = out_weights[g * 4 : (g + 1) * 4, :, cols].reshape(512, 512)
            d = jnp.dot(returned[g], w, preferred_element_type=F32)
            total = d if total is None else total + d
        projected[:, cols] = total
        squares = squares + jnp.sum(total * total, axis=-1, keepdims=True)
    scale = lax.rsqrt(squares * (1.0 / WIDTH) + EPS)
    out[0] = (projected[...] * scale * out_gain[...]).astype(BF16)

    for copy in sent:
        copy.wait_send()


def on_device(tokens, in_gain, wq, wk, wv, q_gain, k_gain, wo, out_gain):
    vmem = pl.BlockSpec(memory_space=pltpu.VMEM)
    dma = pltpu.SemaphoreType.DMA
    return pl.pallas_call(
        kernel,
        out_shape=jax.ShapeDtypeStruct((1, ROWS, WIDTH), BF16),
        in_specs=[vmem] * 9,
        out_specs=vmem,
        scratch_shapes=[
            pltpu.VMEM((3, ROWS, WIDTH), BF16),
            pltpu.VMEM((GROUP, ROWS, WIDTH), BF16),
            pltpu.VMEM((2 * Z, SHARD, CUT), BF16),
            pltpu.VMEM((2 * Z, SHARD, WIDTH), BF16),
            pltpu.VMEM((GROUP, ROWS, HEAD), F32),
            pltpu.VMEM((GROUP, ROWS, HEAD), F32),
            pltpu.VMEM((2 * HEAD, KEYS * GROUP), BF16),
            pltpu.VMEM((GROUP, KEYS, HEAD), BF16),
            pltpu.VMEM((GROUP, HEAD + ONES, KEYS), BF16),
            pltpu.VMEM((KEYS, BQ), F32),
            pltpu.VMEM((KEYS, BQ), F32),
            pltpu.VMEM((8, BQ), F32),
            pltpu.VMEM((8, BQ), F32),
            pltpu.VMEM((1, KEYS * GROUP), F32),
            pltpu.VMEM((HEAD + ONES, KEYS * GROUP), F32),
            pltpu.VMEM((GROUP, ROWS, 512), BF16),
            pltpu.VMEM((GROUP, ROWS, 512), BF16),
            pltpu.VMEM((ROWS, WIDTH), F32),
            dma((6,)),
            dma((6,)),
            dma((2, 4, 2)),
            dma((2, 4, 2)),
            dma((Z, 2)),
            dma((Z, 2)),
            dma((2, 4, 2)),
            dma((2, 4, 2)),
            dma((Z, 2)),
            dma((Z, 2)),
            dma((6,)),
            dma((6,)),
            dma((3,)),
            dma((3,)),
        ],
        compiler_params=pltpu.CompilerParams(
            collective_id=0, has_side_effects=True, vmem_limit_bytes=60 * 2**20
        ),
        name="grouped_attention",
    )(
        tokens,
        in_gain.reshape(1, WIDTH),
        wq,
        wk,
        wv,
        q_gain.reshape(1, HEAD),
        k_gain.reshape(1, HEAD),
        wo,
        out_gain.reshape(1, WIDTH),
    )


def solution(mesh):
    placed = (
        P("dp", "sp", None),
        P(),
        P("dp", None),
        P("dp", None),
        P("dp", None),
        P(),
        P(),
        P("dp", None),
        P(),
    )
    return jax.shard_map(
        on_device, mesh=mesh, in_specs=placed, out_specs=P("dp", "sp", None), check_vma=False
    )
```

time: 248 us -> 92.7 us (0.37)
  waiting for transfers between devices: 108 us -> 0 us
  Pallas kernels: 0 us -> 90.3 us
  matrix products: 59.5 us -> 0 us
  other arithmetic: 26.5 us -> 0 us
  blocking collectives: 21.1 us -> 0 us
  between operations: 13.6 us -> 0.01 us
  starting transfers between devices: 10 us -> 0 us
  local copies, waits for them, and re-layouts: 8.59 us -> 2.3 us
    pallas_call x0 -> x1, Pallas kernels: none -> 90.3 us  [on_device(): pl.pallas_call(kernel, out_shape=jax.ShapeDtypeStruct((1, ROWS, WIDTH), B...]
    all_gather x2 -> x0, waiting for transfers between devices: 69.2 us -> none  [the longest x1 69.2 us: on_device(): shard_rows = lax.all_gather(normed, 'sp', axis=0, tiled=True)]
    dot_general x18 -> x0, matrix products: 59.5 us -> none  [the longest x8 25.1 us: one_block(): jnp.einsum('egqk,ked->qegd', weights, value_heads, preferred_element_type...]
    all_to_all x1 -> x0, waiting for transfers between devices: 37.7 us -> none  [copy_for_each(): lax.all_to_all(jnp.broadcast_to(x[None], (devices, *x.shape)), axis, 0, 0...]
    all_to_all x1 -> x0, blocking collectives: 21.1 us -> none  [on_device(): lax.all_to_all(attended, 'sp', split_axis=0, concat_axis=1, tiled=True)]
    reduce_sum x10 -> x0, other arithmetic: 13.9 us -> none  [the longest x8 12 us: one_block(): jnp.sum(raised, axis=-1, keepdims=True)]
    all_to_all x1 -> x0, starting transfers between devices: 9.97 us -> none  [copy_for_each(): lax.all_to_all(jnp.broadcast_to(x[None], (devices, *x.shape)), axis, 0, 0...]
    while x19 -> x0, local copies, waits for them, and re-layouts: 5.2 us -> none  [the longest x3 5.18 us: attend(): lax.map(one_block, query_block_list)]
  transfers between devices with their start and end apart: 3 -> 0, of which waited for: 2 -> 0; matrix products, arithmetic and copies ran while one was open for 34% -> 0% of each run, Pallas kernels for 0% -> 0%
where the time goes in v1:
time: 92.7 us; the launch traced here: 92.6 us
  Pallas kernels  90.3 us (97%)
  local copies, waits for them, and re-layouts  2.3 us (2%)
    pallas_call x1, Pallas kernels, on_device(): pl.pallas_call(kernel, out_shape=jax.ShapeDtypeStruct((1, ROWS, WIDTH), B...  90.3 us
    unnamed x1, local copies, waits for them, and re-layouts  2.3 us

profile of v1, /device:TPU:1, one launch (start us, length us, event | category | flops | bytes accessed | tf_op | source)
XLA Modules:
  0.0 92.6 jit_solution(563178328891737919)
XLA Ops:
  0.0 90.3 %grouped_attention.1 = bf16[1,256,2048]{2,1,0:T(8,128)(2,1)} custom-call(bf16[1,256,2048]{2,1,0:T(8,128)(2,1)} %tokens.1, f32[1,2048]{1,0:T(1,128)} %bitcast.4, bf16[128,2048]{1,0:T(8,128)(2,1)} %wq.1, bf16[128,512]{1,0:T(8,128)(2,1)} %wk.1, bf16[128,512]{1,0:T(8,128)(2,1)} %wv.1, f32[1,128]{1,0:T(1,128)} %bitcast.6, f32[1,128]{1,0:T(1,128)} %bitcast.7, ...), custom_call_target="tpu_custom_call" | custom-call | tf_op jit(solution)/shard_map/grouped_attention/pallas_call | solution.py:415
  90.3 2.3 %copy.11 = bf16[1,256,2048]{2,1,0:T(8,128)(2,1)} copy(bf16[1,256,2048]{2,1,0:T(8,128)(2,1)} %grouped_attention.1) | data formatting | bytes 2097152

commit v2 on v1

v2 whole, which is shorter than its diff:
```python
import jax
import jax.numpy as jnp
from jax import lax
from jax.experimental import pallas as pl
from jax.experimental.pallas import tpu as pltpu
from jax.sharding import PartitionSpec as P

MESH = pl.DeviceIdType.MESH
F32 = jnp.float32
BF16 = jnp.bfloat16

EPS = 1e-06
THETA = 10000.0
GRID_W = 64
HEAD = 128
WIDTH = 2048
ROWS = 256
GROUP = 4
KEYS = GROUP * ROWS
Z = 8
SHARD = WIDTH // (2 * Z)
NEAR = 1280
SHARED = 512
FAR = 768
HALF = ROWS // 2
BQ = 512
TILES = KEYS * GROUP // BQ
ONES = 16
LOG2E = 1.4426950408889634


def span(index, size):
    return pl.ds(pl.multiple_of(index * size, size), size)


def kernel(
    tokens_in,
    in_gain,
    wq_in,
    wk_in,
    wv_in,
    q_gain,
    k_gain,
    wo_in,
    out_gain,
    out,
    tokens,
    wq,
    wk,
    wv,
    wo,
    raw,
    normed,
    kv_weights,
    q_weights,
    near,
    far,
    cosines,
    sines,
    qt,
    kbuf,
    vbuf,
    s0,
    s1,
    top0,
    top1,
    row_max,
    acc,
    attended,
    returned,
    projected,
    in_sem,
    ag_send,
    ag_recv,
    zk_send,
    zk_recv,
    ck_send,
    ck_recv,
    zq_send,
    zq_recv,
    cq_send,
    cq_recv,
    zo_send,
    zo_recv,
    co_send,
    co_recv,
    far_send,
    far_recv,
    cf_send,
    cf_recv,
    kv_send,
    kv_recv,
    ret_send,
    ret_recv,
):
    staged = []
    for i, (src, dst) in enumerate(
        ((tokens_in.at[0], tokens), (wk_in, wk), (wv_in, wv), (wq_in, wq), (wo_in, wo))
    ):
        staged.append(pltpu.make_async_copy(src, dst, in_sem.at[i]))
        staged[-1].start()

    sp = lax.axis_index("sp")
    dp = lax.axis_index("dp")
    y, x = sp // 4, sp % 4
    z, core = dp // 2, dp % 2
    at = (1 - core) * y + core * x
    group = (y + x) % 4
    side = group % 2

    def member(step):
        to = (at + step) % 4
        return (1 - core) * (to * 4 + x) + core * (y * 4 + to)

    def diagonal(step):
        return ((y + 4 - step) % 4) * 4 + (x + step) % 4

    up = {"dp": ((z + 1) % Z) * 2 + core}
    down = {"dp": ((z + Z - 1) % Z) * 2 + core}
    twin = {"dp": z * 2 + 1 - core}
    peers = [{"sp": member(1)}, {"sp": member(3)}, {"sp": member(2)}]
    peers += [{"sp": diagonal(1)}, {"sp": diagonal(3)}, up, down, twin]

    barrier = pltpu.get_barrier_semaphore()
    for peer in peers:
        pl.semaphore_signal(barrier, inc=1, device_id=peer, device_id_type=MESH)
    for copy in staged:
        copy.wait()
    pl.semaphore_wait(barrier, len(peers))

    sent = []

    def send(src, dst, send_sem, recv_sem, to):
        copy = pltpu.make_async_remote_copy(
            src_ref=src,
            dst_ref=dst,
            send_sem=send_sem,
            recv_sem=recv_sem,
            device_id=to,
            device_id_type=MESH,
        )
        copy.start()
        return copy

    def send_parts(pairs, whole, send_sem, recv_sem, to):
        for src, dst in pairs:
            send(src, dst, send_sem, recv_sem, to)
        sent.append(
            pltpu.make_async_remote_copy(
                src_ref=whole,
                dst_ref=whole,
                send_sem=send_sem,
                recv_sem=recv_sem,
                device_id=to,
                device_id_type=MESH,
            )
        )

    def arrival(ref, sem):
        pltpu.make_async_copy(ref, ref, sem).wait()

    low, high = pl.ds(0, HALF), pl.ds(HALF, HALF)
    nxt, prv = {"sp": member(1)}, {"sp": member(3)}

    def token_send(src, slot, part, index, to):
        sent.append(
            send(src, raw.at[slot - 1, part], ag_send.at[index], ag_recv.at[index], to)
        )

    token_send(tokens.at[low], 3, low, 0, nxt)
    token_send(tokens.at[high], 1, high, 1, prv)
    token_send(tokens.at[high], 3, high, 2, nxt)
    token_send(tokens.at[low], 1, low, 3, prv)

    chunks = (pl.ds(0, SHARD // 2), pl.ds(SHARD // 2, SHARD // 2))
    q_cols = span(group, 512)
    kv_cols = span(group, HEAD)
    side_cols = pl.ds(pl.multiple_of(SHARED + side * FAR, 256), FAR)
    other_cols = pl.ds(pl.multiple_of(SHARED + (1 - side) * FAR, 256), FAR)

    def kv_parts(i):
        mine = kv_weights.at[dp, chunks[i]]
        pairs = [
            (wk.at[chunks[i], kv_cols], mine.at[:, pl.ds(0, HEAD)]),
            (wv.at[chunks[i], kv_cols], mine.at[:, pl.ds(HEAD, HEAD)]),
        ]
        return pairs, mine

    def q_parts(i):
        mine = q_weights.at[dp, chunks[i]]
        return [(wq.at[chunks[i], q_cols], mine)], mine

    def near_parts(i):
        mine = near.at[dp, chunks[i]]
        pairs = [
            (wo.at[chunks[i], pl.ds(0, SHARED)], mine.at[:, pl.ds(0, SHARED)]),
            (wo.at[chunks[i], side_cols], mine.at[:, pl.ds(SHARED, FAR)]),
        ]
        return pairs, mine

    def ring_start(parts, zs, zr):
        for i in (0, 1):
            for way, to in ((0, up), (1, down)):
                send_parts(*parts(i), zs.at[way, 0, i], zr.at[way, 0, i], to)

    def twin_start(parts, cs, cr):
        for i in (0, 1):
            send_parts(*parts(i), cs.at[0, i], cr.at[0, i], twin)

    def source_of(way, step):
        return (((z + Z - step) % Z) if way == 0 else ((z + step) % Z)) * 2 + core

    def slot_of(way, step):
        return step if way == 0 else Z - step

    def ring_event(buf, zs, zr, cs, cr, way, step, i):
        part = buf.at[source_of(way, step), chunks[i]]
        arrival(part, zr.at[way, step - 1, i])
        if step < 3 or (step == 3 and i == way):
            sent.append(
                send(part, part, zs.at[way, step, i], zr.at[way, step, i], (up, down)[way])
            )
        slot = slot_of(way, step)
        sent.append(send(part, part, cs.at[slot, i], cr.at[slot, i], twin))

    def ring_events(ring, step, which=(0, 1)):
        for i in which:
            for way in (0, 1):
                if step < 4 or i == way:
                    ring_event(*ring, way, step, i)

    def twin_arrivals(buf, cr, first=0):
        for slot in range(first, Z):
            source = ((z + Z - slot) % Z) * 2 + 1 - core
            for i in (0, 1):
                arrival(buf.at[source, chunks[i]], cr.at[slot, i])

    kv_ring = (kv_weights, zk_send, zk_recv, ck_send, ck_recv)
    q_ring = (q_weights, zq_send, zq_recv, cq_send, cq_recv)
    near_ring = (near, zo_send, zo_recv, co_send, co_recv)

    ring_start(kv_parts, zk_send, zk_recv)
    ring_start(q_parts, zq_send, zq_recv)
    twin_start(kv_parts, ck_send, ck_recv)
    twin_start(q_parts, cq_send, cq_recv)

    kv_weights[dp, :, 0:HEAD] = wk[:, kv_cols]
    kv_weights[dp, :, HEAD : 2 * HEAD] = wv[:, kv_cols]
    q_weights[dp] = wq[:, q_cols]
    near[dp, :, 0:SHARED] = wo[:, 0:SHARED]
    near[dp, :, SHARED:NEAR] = wo[:, side_cols]
    far[dp] = wo[:, other_cols]

    gain_in = in_gain[...]

    def normalize(src, slot):
        def rows(i, c):
            part = pl.ds(pl.multiple_of(i * 32, 32), 32)
            v = src[part, :].astype(F32)
            ms = jnp.mean(v * v, axis=-1, keepdims=True)
            normed[slot, part, :] = (v * lax.rsqrt(ms + EPS) * gain_in).astype(BF16)
            return c

        lax.fori_loop(0, ROWS // 32, rows, 0)

    def angles(slot, c):
        row = lax.broadcasted_iota(jnp.int32, (ROWS, HEAD), 0)
        lane = lax.broadcasted_iota(jnp.int32, (ROWS, HEAD), 1)
        power = (lane % 32).astype(F32) * (1.0 / 32.0)
        freq = jnp.exp(power * (-9.210340371976184))
        grid_row = member(slot) * (ROWS // GRID_W) + row // GRID_W
        place = jnp.where(lane < 64, grid_row, row % GRID_W).astype(F32)
        angle = place * freq
        cosines[slot] = jnp.cos(angle)
        sine = jnp.sin(angle)
        sines[slot] = jnp.where(lane % 64 < 32, -sine, sine)
        return c

    normalize(tokens, 0)
    ring_events(kv_ring, 1)
    ring_events(q_ring, 1)
    ring_events(kv_ring, 2)
    arrival(raw.at[2, low], ag_recv.at[0])
    token_send(raw.at[2, low], 2, low, 4, nxt)
    arrival(raw.at[0, high], ag_recv.at[1])
    token_send(raw.at[0, high], 2, high, 5, prv)
    ring_events(q_ring, 2)
    lax.fori_loop(0, GROUP, angles, 0)
    ring_events(kv_ring, 3)
    ring_events(q_ring, 3)
    arrival(raw.at[2, high], ag_recv.at[2])
    arrival(raw.at[0, low], ag_recv.at[3])
    normalize(raw.at[0], 1)
    ring_events(kv_ring, 4)
    normalize(raw.at[2], 3)
    ring_events(q_ring, 4)
    ring_start(near_parts, zo_send, zo_recv)
    twin_arrivals(kv_weights, ck_recv)

    gain_q, gain_k = q_gain[...], k_gain[...]
    lane_of = lax.broadcasted_iota(jnp.int32, (ROWS, HEAD), 1)
    first = lane_of % 64 < 32

    def finish(v, gain, slot):
        ms = jnp.mean(v * v, axis=-1, keepdims=True)
        v = v * lax.rsqrt(ms + EPS) * gain
        other = jnp.where(first, pltpu.roll(v, HEAD - 32, 1), pltpu.roll(v, 32, 1))
        return v * cosines[slot] + other * sines[slot]

    def project_kv(slot):
        cut = kv_weights[...].reshape(WIDTH, 2 * HEAD)
        values = jnp.dot(normed[slot], cut, preferred_element_type=F32)
        rows = pl.ds(slot * ROWS, ROWS)
        kbuf[0, rows, :] = finish(values[:, 0:HEAD], gain_k, slot).astype(BF16)
        vbuf[0, 0:HEAD, rows] = values[:, HEAD : 2 * HEAD].T.astype(BF16)

    def kv_part(d, what, half):
        part = pl.ds(half * KEYS // 2, KEYS // 2)
        return kbuf.at[d, part] if what == 0 else vbuf.at[d, pl.ds(0, HEAD), part]

    def kv_index(d, what, half):
        return (d - 1) * 4 + what * 2 + half

    def kv_send_to(src, slot, what, half, to):
        index = kv_index(slot, what, half)
        sent.append(
            send(
                kv_part(src, what, half),
                kv_part(slot, what, half),
                kv_send.at[index],
                kv_recv.at[index],
                {"sp": diagonal(to)},
            )
        )

    def kv_arrival(slot, what, half):
        arrival(kv_part(slot, what, half), kv_recv.at[kv_index(slot, what, half)])

    def kv_out(half):
        kv_send_to(0, 3, 0, half, 1)
        kv_send_to(0, 1, 1, half, 3)
        kv_send_to(0, 3, 1, half, 1)
        kv_send_to(0, 1, 0, half, 3)

    def kv_pass(half):
        kv_arrival(3, 0, half)
        kv_send_to(3, 2, 0, half, 1)
        kv_arrival(1, 1, half)
        kv_send_to(1, 2, 1, half, 3)

    project_kv(0)
    project_kv(1)
    kv_out(0)
    arrival(raw.at[1, low], ag_recv.at[4])
    arrival(raw.at[1, high], ag_recv.at[5])
    normalize(raw.at[1], 2)
    project_kv(3)
    project_kv(2)
    kv_out(1)
    twin_arrivals(q_weights, cq_recv)
    twin_start(near_parts, co_send, co_recv)
    for i in (0, 1):
        part = far.at[dp, chunks[i]]
        sent.append(
            send(wo.at[chunks[i], other_cols], part, cf_send.at[0, i], cf_recv.at[0, i], twin)
        )

    def project_q(slot, c):
        cut = q_weights[...].reshape(WIDTH, 512)
        values = jnp.dot(normed[slot], cut, preferred_element_type=F32)
        for h in range(4):
            q = finish(values[:, h * HEAD : (h + 1) * HEAD], gain_q, slot)
            q = q.astype(BF16).astype(F32).T * (HEAD**-0.5 * LOG2E)
            coarse = q.astype(BF16)
            fine = (q - coarse.astype(F32)).astype(BF16)
            cols = pl.ds(pl.multiple_of(slot * KEYS + h * ROWS, ROWS), ROWS)
            qt[0:HEAD, cols] = coarse
            qt[HEAD : 2 * HEAD, cols] = fine
        return c

    lax.fori_loop(0, GROUP, project_q, 0)

    def far_out(step, i):
        for way in (0, 1):
            if step < 4 or i == way:
                source, slot = source_of(way, step), slot_of(way, step)
                sent.append(
                    send(
                        near.at[source, chunks[i], pl.ds(SHARED, FAR)],
                        far.at[source, chunks[i]],
                        far_send.at[slot, i],
                        far_recv.at[slot, i],
                        (nxt, prv)[i],
                    )
                )

    def far_pass(step, i):
        for way in (0, 1):
            if step < 4 or i == way:
                slot = slot_of(way, step)
                part = far.at[source_of(way, step), chunks[i]]
                arrival(part, far_recv.at[slot, i])
                sent.append(send(part, part, cf_send.at[slot, i], cf_recv.at[slot, i], twin))

    ones = jnp.ones((ONES, KEYS), BF16)
    for d in range(GROUP):
        vbuf[d, HEAD : HEAD + ONES, :] = ones
    row_max[...] = jnp.full_like(row_max, -1e30)
    acc[...] = jnp.zeros_like(acc)
    size = 256

    def attend(nt, sn, topn, next_keys, ct, sc, topc, keys):
        if sc is not None:
            cols = span(ct, BQ)
            old = row_max[:, cols]
            new = jnp.maximum(old, jnp.max(topc[...], axis=0, keepdims=True))
            row_max[:, cols] = new
            decay = jnp.exp2(old - new)
        top, total = None, None
        for c in range(KEYS // size):
            part = pl.ds(c * size, size)
            if sn is not None:
                d, begin = next_keys[c]
                k = kbuf[d, pl.ds(begin, size), :]
                s = jnp.dot(
                    jnp.concatenate([k, k], axis=1),
                    qt[:, span(nt, BQ)],
                    preferred_element_type=F32,
                )
                sn[part, :] = s
                most = jnp.max(s.reshape(size // 8, 8, BQ), axis=0)
                top = most if top is None else jnp.maximum(top, most)
            if sc is not None:
                d, begin = keys[c]
                p = jnp.exp2(sc[part, :] - new).astype(BF16)
                v = jnp.dot(
                    vbuf[d, :, pl.ds(begin, size)], p, preferred_element_type=F32
                )
                total = v if total is None else total + v
        if sn is not None:
            topn[...] = top
        if sc is not None:
            acc[:, cols] = acc[:, cols] * decay + total

    def attend_block(keys, next_keys, middle, late):
        def pair(i, c):
            t = i * 2
            attend(t + 1, s1, top1, keys, t, s0, top0, keys)
            attend(t + 2, s0, top0, keys, t + 1, s1, top1, keys)
            return c

        lax.fori_loop(0, TILES // 4, pair, 0)
        middle()
        lax.fori_loop(TILES // 4, TILES // 2 - 1, pair, 0)
        late()
        t = TILES - 2
        attend(t + 1, s1, top1, keys, t, s0, top0, keys)
        if next_keys is None:
            attend(None, None, None, None, t + 1, s1, top1, keys)
        else:
            attend(0, s0, top0, next_keys, t + 1, s1, top1, keys)

    quarters = [i * size for i in range(KEYS // size)]
    own = [(0, i) for i in quarters]
    firsts = [(3, i) for i in quarters[:2]] + [(1, i) for i in quarters[:2]]
    seconds = [(3, i) for i in quarters[2:]] + [(1, i) for i in quarters[2:]]
    opposite = [(2, i) for i in quarters]

    attend(0, s0, top0, own, None, None, None, None)

    def middle0():
        ring_events(near_ring, 1, (0,))

    def late0():
        kv_pass(0)
        kv_arrival(3, 1, 0)
        kv_arrival(1, 0, 0)

    attend_block(own, firsts, middle0, late0)
    ring_events(near_ring, 1, (1,))

    def middle1():
        ring_events(near_ring, 2, (0,))

    def late1():
        kv_pass(1)
        kv_arrival(3, 1, 1)
        kv_arrival(1, 0, 1)
        far_out(1, 0)
        far_out(1, 1)

    attend_block(firsts, seconds, middle1, late1)

    def middle2():
        ring_events(near_ring, 2, (1,))
        far_out(2, 0)
        far_out(2, 1)

    def late2():
        ring_events(near_ring, 3, (0,))
        for half in (0, 1):
            kv_arrival(2, 0, half)
            kv_arrival(2, 1, half)

    attend_block(seconds, opposite, middle2, late2)

    def middle3():
        far_out(3, 0)

    def late3():
        ring_events(near_ring, 3, (1,))
        far_out(3, 1)
        for i in (0, 1):
            far_pass(1, i)

    attend_block(opposite, None, middle3, late3)

    def hand_back(slot):
        for h in range(4):
            cols = pl.ds(slot * KEYS + h * ROWS, ROWS)
            scaled = acc[0:HEAD, cols] / acc[HEAD : HEAD + 1, cols]
            attended[slot, :, h * HEAD : (h + 1) * HEAD] = scaled.T.astype(BF16)

    for slot in (2, 1, 3):
        hand_back(slot)
        sent.append(
            send(
                attended.at[slot],
                returned.at[group],
                ret_send.at[slot - 1],
                ret_recv.at[slot - 1],
                {"sp": member(slot)},
            )
        )
    hand_back(0)
    returned[group] = attended[0]
    ring_events(near_ring, 4)
    far_out(4, 0)
    far_out(4, 1)
    for step in (2, 3, 4):
        for i in (0, 1):
            far_pass(step, i)
    for slot in (1, 2, 3):
        arrival(returned.at[(group + 4 - slot) % 4], ret_recv.at[slot - 1])
    twin_arrivals(near, co_recv)

    def project_out(buf, begin, width):
        total = None
        for g in range(4):
            w = buf[g * 4 : (g + 1) * 4, :, begin : begin + width].reshape(512, width)
            d = jnp.dot(returned[g], w, preferred_element_type=F32)
            total = d if total is None else total + d
        return total, jnp.sum(total * total, axis=-1, keepdims=True)

    total, squares = project_out(near, 0, SHARED)
    projected[:, 0:SHARED] = total
    total, more = project_out(near, SHARED, FAR)
    projected[:, side_cols] = total
    squares = squares + more
    twin_arrivals(far, cf_recv)
    total, more = project_out(far, 0, FAR)
    projected[:, other_cols] = total
    squares = squares + more
    scale = lax.rsqrt(squares * (1.0 / WIDTH) + EPS)
    out[0] = (projected[...] * scale * out_gain[...]).astype(BF16)

    for copy in sent:
        copy.wait_send()


def on_device(tokens, in_gain, wq, wk, wv, q_gain, k_gain, wo, out_gain):
    vmem = pl.BlockSpec(memory_space=pltpu.VMEM)
    hbm = pl.BlockSpec(memory_space=pl.ANY)
    dma = pltpu.SemaphoreType.DMA
    ring, other_core = dma((2, 4, 2)), dma((Z, 2))
    return pl.pallas_call(
        kernel,
        out_shape=jax.ShapeDtypeStruct((1, ROWS, WIDTH), BF16),
        in_specs=[hbm, vmem, hbm, hbm, hbm, vmem, vmem, hbm, vmem],
        out_specs=vmem,
        scratch_shapes=[
            pltpu.VMEM((ROWS, WIDTH), BF16),
            pltpu.VMEM(wq.shape, BF16),
            pltpu.VMEM(wk.shape, BF16),
            pltpu.VMEM(wv.shape, BF16),
            pltpu.VMEM(wo.shape, BF16),
            pltpu.VMEM((3, ROWS, WIDTH), BF16),
            pltpu.VMEM((GROUP, ROWS, WIDTH), BF16),
            pltpu.VMEM((2 * Z, SHARD, 2 * HEAD), BF16),
            pltpu.VMEM((2 * Z, SHARD, 512), BF16),
            pltpu.VMEM((2 * Z, SHARD, NEAR), BF16),
            pltpu.VMEM((2 * Z, SHARD, FAR), BF16),
            pltpu.VMEM((GROUP, ROWS, HEAD), F32),
            pltpu.VMEM((GROUP, ROWS, HEAD), F32),
            pltpu.VMEM((2 * HEAD, KEYS * GROUP), BF16),
            pltpu.VMEM((GROUP, KEYS, HEAD), BF16),
            pltpu.VMEM((GROUP, HEAD + ONES, KEYS), BF16),
            pltpu.VMEM((KEYS, BQ), F32),
            pltpu.VMEM((KEYS, BQ), F32),
            pltpu.VMEM((8, BQ), F32),
            pltpu.VMEM((8, BQ), F32),
            pltpu.VMEM((1, KEYS * GROUP), F32),
            pltpu.VMEM((HEAD + ONES, KEYS * GROUP), F32),
            pltpu.VMEM((GROUP, ROWS, 512), BF16),
            pltpu.VMEM((GROUP, ROWS, 512), BF16),
            pltpu.VMEM((ROWS, WIDTH), F32),
            dma((5,)),
            dma((6,)),
            dma((6,)),
            *([ring, ring, other_core, other_core] * 3),
            *([other_core] * 4),
            dma((12,)),
            dma((12,)),
            dma((3,)),
            dma((3,)),
        ],
        compiler_params=pltpu.CompilerParams(
            collective_id=0, has_side_effects=True, vmem_limit_bytes=60 * 2**20
        ),
        name="grouped_attention",
    )(
        tokens,
        in_gain.reshape(1, WIDTH),
        wq,
        wk,
        wv,
        q_gain.reshape(1, HEAD),
        k_gain.reshape(1, HEAD),
        wo,
        out_gain.reshape(1, WIDTH),
    )


def solution(mesh):
    placed = (
        P("dp", "sp", None),
        P(),
        P("dp", None),
        P("dp", None),
        P("dp", None),
        P(),
        P(),
        P("dp", None),
        P(),
    )
    return jax.shard_map(
        on_device, mesh=mesh, in_specs=placed, out_specs=P("dp", "sp", None), check_vma=False
    )
```

time: 92.7 us -> 82.7 us (0.89)
  Pallas kernels: 90.3 us -> 80.2 us
    pallas_call x1, Pallas kernels: 90.3 us -> 80.2 us  [on_device(): pl.pallas_call(kernel, out_shape=jax.ShapeDtypeStruct((1, ROWS, WIDTH), B...]
where the time goes in v2:
time: 82.7 us; the launch traced here: 82.5 us
  Pallas kernels  80.2 us (97%)
  local copies, waits for them, and re-layouts  2.3 us (3%)
    pallas_call x1, Pallas kernels, on_device(): pl.pallas_call(kernel, out_shape=jax.ShapeDtypeStruct((1, ROWS, WIDTH), B...  80.2 us
    unnamed x1, local copies, waits for them, and re-layouts  2.3 us

profile of v2, /device:TPU:1, one launch (start us, length us, event | category | flops | bytes accessed | tf_op | source)
XLA Modules:
  0.0 82.5 jit_solution(10867253714314505146)
XLA Ops:
  0.0 80.2 %grouped_attention.1 = bf16[1,256,2048]{2,1,0:T(8,128)(2,1)} custom-call(bf16[1,256,2048]{2,1,0:T(8,128)(2,1)} %tokens_in.1, f32[1,2048]{1,0:T(1,128)} %bitcast.4, bf16[128,2048]{1,0:T(8,128)(2,1)} %wq_in.1, bf16[128,512]{1,0:T(8,128)(2,1)} %wk_in.1, bf16[128,512]{1,0:T(8,128)(2,1)} %wv_in.1, f32[1,128]{1,0:T(1,128)} %bitcast.6, f32[1,128]{1,0:T(1,128)} %bitcast.7, ...), custom_call_target="tpu_custom_call" | custom-call | tf_op jit(solution)/shard_map/grouped_attention/pallas_call | solution.py:576
  80.2 2.3 %copy.11 = bf16[1,256,2048]{2,1,0:T(8,128)(2,1)} copy(bf16[1,256,2048]{2,1,0:T(8,128)(2,1)} %grouped_attention.1) | data formatting | bytes 2097152

commit v3 on v2

--- a/solution.py
+++ b/solution.py
@@ -35,15 +35,19 @@
 
 def kernel(
     tokens_in,
-    in_gain,
+    in_gain_in,
     wq_in,
     wk_in,
     wv_in,
+    q_gain_in,
+    k_gain_in,
+    wo_in,
+    out_gain_in,
+    out,
+    in_gain,
     q_gain,
     k_gain,
-    wo_in,
     out_gain,
-    out,
     tokens,
     wq,
     wk,
@@ -57,6 +61,8 @@
     far,
     cosines,
     sines,
+    cosines_t,
+    sines_t,
     qt,
     kbuf,
     vbuf,
@@ -95,7 +101,17 @@
 ):
     staged = []
     for i, (src, dst) in enumerate(
-        ((tokens_in.at[0], tokens), (wk_in, wk), (wv_in, wv), (wq_in, wq), (wo_in, wo))
+        (
+            (tokens_in.at[0], tokens),
+            (wk_in, wk),
+            (wv_in, wv),
+            (wq_in, wq),
+            (wo_in, wo),
+            (in_gain_in, in_gain),
+            (q_gain_in, q_gain),
+            (k_gain_in, k_gain),
+            (out_gain_in, out_gain),
+        )
     ):
         staged.append(pltpu.make_async_copy(src, dst, in_sem.at[i]))
         staged[-1].start()
@@ -124,7 +140,7 @@
     barrier = pltpu.get_barrier_semaphore()
     for peer in peers:
         pl.semaphore_signal(barrier, inc=1, device_id=peer, device_id_type=MESH)
-    for copy in staged:
+    for copy in staged[:4]:
         copy.wait()
     pl.semaphore_wait(barrier, len(peers))
 
@@ -244,6 +260,8 @@
     twin_start(kv_parts, ck_send, ck_recv)
     twin_start(q_parts, cq_send, cq_recv)
 
+    for copy in staged[4:]:
+        copy.wait()
     kv_weights[dp, :, 0:HEAD] = wk[:, kv_cols]
     kv_weights[dp, :, HEAD : 2 * HEAD] = wv[:, kv_cols]
     q_weights[dp] = wq[:, q_cols]
@@ -271,9 +289,13 @@
         grid_row = member(slot) * (ROWS // GRID_W) + row // GRID_W
         place = jnp.where(lane < 64, grid_row, row % GRID_W).astype(F32)
         angle = place * freq
-        cosines[slot] = jnp.cos(angle)
+        cosine = jnp.cos(angle)
         sine = jnp.sin(angle)
-        sines[slot] = jnp.where(lane % 64 < 32, -sine, sine)
+        sine = jnp.where(lane % 64 < 32, -sine, sine)
+        cosines[slot] = cosine
+        sines[slot] = sine
+        cosines_t[slot] = cosine.T
+        sines_t[slot] = sine.T
         return c
 
     normalize(tokens, 0)
@@ -365,12 +387,18 @@
             send(wo.at[chunks[i], other_cols], part, cf_send.at[0, i], cf_recv.at[0, i], twin)
         )
 
+    gain_rows = jnp.broadcast_to(gain_q, (HEAD, HEAD)).T[:, 0:1]
+
     def project_q(slot, c):
         cut = q_weights[...].reshape(WIDTH, 512)
         values = jnp.dot(normed[slot], cut, preferred_element_type=F32)
         for h in range(4):
-            q = finish(values[:, h * HEAD : (h + 1) * HEAD], gain_q, slot)
-            q = q.astype(BF16).astype(F32).T * (HEAD**-0.5 * LOG2E)
+            v = values[:, h * HEAD : (h + 1) * HEAD].T
+            ms = jnp.mean(v * v, axis=0, keepdims=True)
+            v = v * lax.rsqrt(ms + EPS) * gain_rows
+            other = jnp.concatenate([v[32:64], v[0:32], v[96:128], v[64:96]], axis=0)
+            q = v * cosines_t[slot] + other * sines_t[slot]
+            q = q.astype(BF16).astype(F32) * (HEAD**-0.5 * LOG2E)
             coarse = q.astype(BF16)
             fine = (q - coarse.astype(F32)).astype(BF16)
             cols = pl.ds(pl.multiple_of(slot * KEYS + h * ROWS, ROWS), ROWS)
@@ -378,7 +406,10 @@
             qt[HEAD : 2 * HEAD, cols] = fine
         return c
 
-    lax.fori_loop(0, GROUP, project_q, 0)
+    lax.fori_loop(0, 2, project_q, 0)
+    ring_events(near_ring, 1, (0,))
+    lax.fori_loop(2, GROUP, project_q, 0)
+    ring_events(near_ring, 1, (1,))
 
     def far_out(step, i):
         for way in (0, 1):
@@ -442,7 +473,7 @@
         if sc is not None:
             acc[:, cols] = acc[:, cols] * decay + total
 
-    def attend_block(keys, next_keys, middle, late):
+    def attend_block(keys, next_keys, next_tile, middle, late):
         def pair(i, c):
             t = i * 2
             attend(t + 1, s1, top1, keys, t, s0, top0, keys)
@@ -455,111 +486,122 @@
         late()
         t = TILES - 2
         attend(t + 1, s1, top1, keys, t, s0, top0, keys)
-        if next_keys is None:
-            attend(None, None, None, None, t + 1, s1, top1, keys)
-        else:
-            attend(0, s0, top0, next_keys, t + 1, s1, top1, keys)
+        attend(next_tile, s0, top0, next_keys, t + 1, s1, top1, keys)
 
     quarters = [i * size for i in range(KEYS // size)]
     own = [(0, i) for i in quarters]
     firsts = [(3, i) for i in quarters[:2]] + [(1, i) for i in quarters[:2]]
     seconds = [(3, i) for i in quarters[2:]] + [(1, i) for i in quarters[2:]]
     opposite = [(2, i) for i in quarters]
+    slots = (2, 1, 3, 0)
 
     attend(0, s0, top0, own, None, None, None, None)
 
     def middle0():
-        ring_events(near_ring, 1, (0,))
+        ring_events(near_ring, 2, (0,))
 
     def late0():
         kv_pass(0)
         kv_arrival(3, 1, 0)
         kv_arrival(1, 0, 0)
-
-    attend_block(own, firsts, middle0, late0)
-    ring_events(near_ring, 1, (1,))
+        far_out(1, 0)
+        far_out(1, 1)
+
+    attend_block(own, firsts, 0, middle0, late0)
 
     def middle1():
-        ring_events(near_ring, 2, (0,))
+        ring_events(near_ring, 2, (1,))
 
     def late1():
+        ring_events(near_ring, 3, (0,))
         kv_pass(1)
         kv_arrival(3, 1, 1)
         kv_arrival(1, 0, 1)
-        far_out(1, 0)
-        far_out(1, 1)
-
-    attend_block(firsts, seconds, middle1, late1)
-
-    def middle2():
-        ring_events(near_ring, 2, (1,))
         far_out(2, 0)
         far_out(2, 1)
 
+    attend_block(firsts, seconds, 0, middle1, late1)
+
+    def middle2():
+        ring_events(near_ring, 3, (1,))
+        far_pass(1, 0)
+        far_pass(1, 1)
+        far_out(3, 0)
+
     def late2():
-        ring_events(near_ring, 3, (0,))
         for half in (0, 1):
             kv_arrival(2, 0, half)
             kv_arrival(2, 1, half)
-
-    attend_block(seconds, opposite, middle2, late2)
-
-    def middle3():
-        far_out(3, 0)
-
-    def late3():
-        ring_events(near_ring, 3, (1,))
         far_out(3, 1)
-        for i in (0, 1):
-            far_pass(1, i)
-
-    attend_block(opposite, None, middle3, late3)
+
+    attend_block(seconds, opposite, 2 * slots[0], middle2, late2)
+
+    ring_events(near_ring, 4)
+    far_out(4, 0)
+    far_out(4, 1)
+    far_pass(2, 0)
+    far_pass(2, 1)
 
     def hand_back(slot):
         for h in range(4):
             cols = pl.ds(slot * KEYS + h * ROWS, ROWS)
             scaled = acc[0:HEAD, cols] / acc[HEAD : HEAD + 1, cols]
             attended[slot, :, h * HEAD : (h + 1) * HEAD] = scaled.T.astype(BF16)
-
-    for slot in (2, 1, 3):
+        if slot:
+            sent.append(
+                send(
+                    attended.at[slot],
+                    returned.at[group],
+                    ret_send.at[slot - 1],
+                    ret_recv.at[slot - 1],
+                    {"sp": member(slot)},
+                )
+            )
+        else:
+            returned[group] = attended[0]
+
+    for n, slot in enumerate(slots):
+        t = 2 * slot
+        after = 2 * slots[n + 1] if n < 3 else None
+        attend(t + 1, s1, top1, opposite, t, s0, top0, opposite)
+        attend(after, None if after is None else s0, top0, opposite, t + 1, s1, top1, opposite)
         hand_back(slot)
-        sent.append(
-            send(
-                attended.at[slot],
-                returned.at[group],
-                ret_send.at[slot - 1],
-                ret_recv.at[slot - 1],
-                {"sp": member(slot)},
-            )
-        )
-    hand_back(0)
-    returned[group] = attended[0]
-    ring_events(near_ring, 4)
-    far_out(4, 0)
-    far_out(4, 1)
-    for step in (2, 3, 4):
-        for i in (0, 1):
-            far_pass(step, i)
+        if n == 1:
+            far_pass(3, 0)
+            far_pass(3, 1)
+    for i in (0, 1):
+        far_pass(4, i)
     for slot in (1, 2, 3):
         arrival(returned.at[(group + 4 - slot) % 4], ret_recv.at[slot - 1])
     twin_arrivals(near, co_recv)
 
-    def project_out(buf, begin, width):
+    def project_out(columns):
         total = None
         for g in range(4):
-            w = buf[g * 4 : (g + 1) * 4, :, begin : begin + width].reshape(512, width)
+            w = [
+                buf[g * 4 : (g + 1) * 4, :, begin : begin + width].reshape(512, width)
+                for buf, begin, width in columns
+            ]
+            w = w[0] if len(w) == 1 else jnp.concatenate(w, axis=1)
             d = jnp.dot(returned[g], w, preferred_element_type=F32)
             total = d if total is None else total + d
         return total, jnp.sum(total * total, axis=-1, keepdims=True)
 
-    total, squares = project_out(near, 0, SHARED)
+    def side_of(which, begin, width):
+        return pl.ds(pl.multiple_of(SHARED + which * FAR + begin, 256), width)
+
+    total, squares = project_out([(near, 0, 512)])
     projected[:, 0:SHARED] = total
-    total, more = project_out(near, SHARED, FAR)
-    projected[:, side_cols] = total
+    total, more = project_out([(near, SHARED, 512)])
+    projected[:, side_of(side, 0, 512)] = total
     squares = squares + more
     twin_arrivals(far, cf_recv)
-    total, more = project_out(far, 0, FAR)
-    projected[:, other_cols] = total
+    total, more = project_out([(far, 0, 512)])
+    projected[:, side_of(1 - side, 0, 512)] = total
+    squares = squares + more
+    total, more = project_out([(near, SHARED + 512, 256), (far, 512, 256)])
+    projected[:, side_of(side, 512, 256)] = total[:, 0:256]
+    projected[:, side_of(1 - side, 512, 256)] = total[:, 256:512]
     squares = squares + more
     scale = lax.rsqrt(squares * (1.0 / WIDTH) + EPS)
     out[0] = (projected[...] * scale * out_gain[...]).astype(BF16)
@@ -576,9 +618,13 @@
     return pl.pallas_call(
         kernel,
         out_shape=jax.ShapeDtypeStruct((1, ROWS, WIDTH), BF16),
-        in_specs=[hbm, vmem, hbm, hbm, hbm, vmem, vmem, hbm, vmem],
+        in_specs=[hbm] * 9,
         out_specs=vmem,
         scratch_shapes=[
+            pltpu.VMEM((1, WIDTH), F32),
+            pltpu.VMEM((1, HEAD), F32),
+            pltpu.VMEM((1, HEAD), F32),
+            pltpu.VMEM((1, WIDTH), F32),
             pltpu.VMEM((ROWS, WIDTH), BF16),
             pltpu.VMEM(wq.shape, BF16),
             pltpu.VMEM(wk.shape, BF16),
@@ -592,6 +638,8 @@
             pltpu.VMEM((2 * Z, SHARD, FAR), BF16),
             pltpu.VMEM((GROUP, ROWS, HEAD), F32),
             pltpu.VMEM((GROUP, ROWS, HEAD), F32),
+            pltpu.VMEM((GROUP, HEAD, ROWS), F32),
+            pltpu.VMEM((GROUP, HEAD, ROWS), F32),
             pltpu.VMEM((2 * HEAD, KEYS * GROUP), BF16),
             pltpu.VMEM((GROUP, KEYS, HEAD), BF16),
             pltpu.VMEM((GROUP, HEAD + ONES, KEYS), BF16),
@@ -604,7 +652,7 @@
             pltpu.VMEM((GROUP, ROWS, 512), BF16),
             pltpu.VMEM((GROUP, ROWS, 512), BF16),
             pltpu.VMEM((ROWS, WIDTH), F32),
-            dma((5,)),
+            dma((9,)),
             dma((6,)),
             dma((6,)),
             *([ring, ring, other_core, other_core] * 3),

time: 82.7 us -> 75.9 us (0.918)
  the two profiles are of different devices: /device:TPU:1 before, /device:TPU:22 now
where the time goes in v3:
time: 75.9 us; the launch traced here: 75.8 us
  Pallas kernels  73.4 us (97%)
  local copies, waits for them, and re-layouts  2.3 us (3%)
    pallas_call x1, Pallas kernels, on_device(): pl.pallas_call(kernel, out_shape=jax.ShapeDtypeStruct((1, ROWS, WIDTH), B...  73.4 us
    unnamed x1, local copies, waits for them, and re-layouts  2.3 us

profile of v3, /device:TPU:22, one launch (start us, length us, event | category | flops | bytes accessed | tf_op | source)
XLA Modules:
  0.0 75.8 jit_solution(4366008984842844443)
XLA Ops:
  0.0 73.4 %grouped_attention.1 = bf16[1,256,2048]{2,1,0:T(8,128)(2,1)} custom-call(bf16[1,256,2048]{2,1,0:T(8,128)(2,1)} %tokens_in.1, f32[1,2048]{1,0:T(1,128)} %bitcast.4, bf16[128,2048]{1,0:T(8,128)(2,1)} %wq_in.1, bf16[128,512]{1,0:T(8,128)(2,1)} %wk_in.1, bf16[128,512]{1,0:T(8,128)(2,1)} %wv_in.1, f32[1,128]{1,0:T(1,128)} %bitcast.6, f32[1,128]{1,0:T(1,128)} %bitcast.7, ...), custom_call_target="tpu_custom_call" | custom-call | tf_op jit(solution)/shard_map/grouped_attention/pallas_call | solution.py:618
  73.5 2.3 %copy.11 = bf16[1,256,2048]{2,1,0:T(8,128)(2,1)} copy(bf16[1,256,2048]{2,1,0:T(8,128)(2,1)} %grouped_attention.1) | data formatting | bytes 2097152

commit v4 on v3

--- a/solution.py
+++ b/solution.py
@@ -75,7 +75,9 @@
     attended,
     returned,
     projected,
+    mixed,
     in_sem,
+    out_sem,
     ag_send,
     ag_recv,
     zk_send,
@@ -215,8 +217,9 @@
         return pairs, mine
 
     def ring_start(parts, zs, zr):
-        for i in (0, 1):
+        for turn in (0, 1):
             for way, to in ((0, up), (1, down)):
+                i = turn ^ way
                 send_parts(*parts(i), zs.at[way, 0, i], zr.at[way, 0, i], to)
 
     def twin_start(parts, cs, cr):
@@ -239,11 +242,11 @@
         slot = slot_of(way, step)
         sent.append(send(part, part, cs.at[slot, i], cr.at[slot, i], twin))
 
-    def ring_events(ring, step, which=(0, 1)):
-        for i in which:
+    def ring_events(ring, step, turns=(0, 1)):
+        for turn in turns:
             for way in (0, 1):
-                if step < 4 or i == way:
-                    ring_event(*ring, way, step, i)
+                if step < 4 or turn == 0:
+                    ring_event(*ring, way, step, turn ^ way)
 
     def twin_arrivals(buf, cr, first=0):
         for slot in range(first, Z):
@@ -438,7 +441,7 @@
         vbuf[d, HEAD : HEAD + ONES, :] = ones
     row_max[...] = jnp.full_like(row_max, -1e30)
     acc[...] = jnp.zeros_like(acc)
-    size = 256
+    size = 512
 
     def attend(nt, sn, topn, next_keys, ct, sc, topc, keys):
         if sc is not None:
@@ -473,145 +476,166 @@
         if sc is not None:
             acc[:, cols] = acc[:, cols] * decay + total
 
-    def attend_block(keys, next_keys, next_tile, middle, late):
-        def pair(i, c):
-            t = i * 2
-            attend(t + 1, s1, top1, keys, t, s0, top0, keys)
-            attend(t + 2, s0, top0, keys, t + 1, s1, top1, keys)
-            return c
-
-        lax.fori_loop(0, TILES // 4, pair, 0)
-        middle()
-        lax.fori_loop(TILES // 4, TILES // 2 - 1, pair, 0)
-        late()
-        t = TILES - 2
-        attend(t + 1, s1, top1, keys, t, s0, top0, keys)
-        attend(next_tile, s0, top0, next_keys, t + 1, s1, top1, keys)
-
-    quarters = [i * size for i in range(KEYS // size)]
-    own = [(0, i) for i in quarters]
-    firsts = [(3, i) for i in quarters[:2]] + [(1, i) for i in quarters[:2]]
-    seconds = [(3, i) for i in quarters[2:]] + [(1, i) for i in quarters[2:]]
-    opposite = [(2, i) for i in quarters]
-    slots = (2, 1, 3, 0)
-
-    attend(0, s0, top0, own, None, None, None, None)
-
-    def middle0():
-        ring_events(near_ring, 2, (0,))
-
-    def late0():
+    def hand_back(tile):
+        slot, part = tile // 2, tile % 2
+        two = pl.ds(part * 2 * HEAD, 2 * HEAD)
+        for h in (0, 1):
+            cols = pl.ds(tile * BQ + h * ROWS, ROWS)
+            scaled = acc[0:HEAD, cols] / acc[HEAD : HEAD + 1, cols]
+            begin = (part * 2 + h) * HEAD
+            attended[slot, :, begin : begin + HEAD] = scaled.T.astype(BF16)
+        if slot:
+            sent.append(
+                send(
+                    attended.at[slot, :, two],
+                    returned.at[group, :, two],
+                    ret_send.at[slot - 1, part],
+                    ret_recv.at[slot - 1, part],
+                    {"sp": member(slot)},
+                )
+            )
+        else:
+            returned[group, :, two] = attended[0, :, two]
+
+    blocks = (
+        ((0, 0), (0, size)),
+        ((3, 0), (1, 0)),
+        ((3, size), (1, size)),
+        ((2, 0), (2, size)),
+    )
+    steps = [(keys, tile) for keys in blocks[:3] for tile in range(TILES)]
+    steps += [(blocks[3], tile) for tile in (4, 5, 2, 3, 6, 7, 0, 1)]
+    buffers = ((s0, top0), (s1, top1))
+
+    def keys_first():
         kv_pass(0)
         kv_arrival(3, 1, 0)
         kv_arrival(1, 0, 0)
         far_out(1, 0)
         far_out(1, 1)
 
-    attend_block(own, firsts, 0, middle0, late0)
-
-    def middle1():
-        ring_events(near_ring, 2, (1,))
-
-    def late1():
-        ring_events(near_ring, 3, (0,))
+    def keys_second():
         kv_pass(1)
         kv_arrival(3, 1, 1)
         kv_arrival(1, 0, 1)
         far_out(2, 0)
         far_out(2, 1)
 
-    attend_block(firsts, seconds, 0, middle1, late1)
-
-    def middle2():
-        ring_events(near_ring, 3, (1,))
-        far_pass(1, 0)
-        far_pass(1, 1)
-        far_out(3, 0)
-
-    def late2():
+    def keys_opposite():
         for half in (0, 1):
             kv_arrival(2, 0, half)
             kv_arrival(2, 1, half)
-        far_out(3, 1)
-
-    attend_block(seconds, opposite, 2 * slots[0], middle2, late2)
-
-    ring_events(near_ring, 4)
-    far_out(4, 0)
-    far_out(4, 1)
-    far_pass(2, 0)
-    far_pass(2, 1)
-
-    def hand_back(slot):
-        for h in range(4):
-            cols = pl.ds(slot * KEYS + h * ROWS, ROWS)
-            scaled = acc[0:HEAD, cols] / acc[HEAD : HEAD + 1, cols]
-            attended[slot, :, h * HEAD : (h + 1) * HEAD] = scaled.T.astype(BF16)
-        if slot:
-            sent.append(
-                send(
-                    attended.at[slot],
-                    returned.at[group],
-                    ret_send.at[slot - 1],
-                    ret_recv.at[slot - 1],
-                    {"sp": member(slot)},
-                )
-            )
+
+    def near_event(step, turns):
+        ring_events(near_ring, step, turns)
+        if step == 3 and turns == (1,):
+            far_out(3, 0)
+            far_out(3, 1)
+            far_pass(1, 0)
+            far_pass(1, 1)
+        if step == 4:
+            far_out(4, 0)
+            far_out(4, 1)
+            far_pass(2, 0)
+            far_pass(2, 1)
+
+    def far_third():
+        far_pass(3, 0)
+        far_pass(3, 1)
+
+    events = {
+        3: [lambda: near_event(2, (0,))],
+        6: [keys_first],
+        10: [lambda: near_event(2, (1,))],
+        13: [lambda: near_event(3, (0,))],
+        14: [keys_second],
+        19: [lambda: near_event(3, (1,))],
+        22: [keys_opposite],
+        25: [lambda: near_event(4, (0,))],
+        28: [far_third],
+    }
+
+    attend(steps[0][1], *buffers[0], steps[0][0], None, None, None, None)
+    for n, (keys, tile) in enumerate(steps):
+        now, later = buffers[n % 2], buffers[(n + 1) % 2]
+        if n + 1 < len(steps):
+            next_keys, next_tile = steps[n + 1]
+            attend(next_tile, *later, next_keys, tile, *now, keys)
         else:
-            returned[group] = attended[0]
-
-    for n, slot in enumerate(slots):
-        t = 2 * slot
-        after = 2 * slots[n + 1] if n < 3 else None
-        attend(t + 1, s1, top1, opposite, t, s0, top0, opposite)
-        attend(after, None if after is None else s0, top0, opposite, t + 1, s1, top1, opposite)
-        hand_back(slot)
-        if n == 1:
-            far_pass(3, 0)
-            far_pass(3, 1)
+            attend(None, None, None, None, tile, *now, keys)
+        if n >= 24:
+            hand_back(tile)
+        for event in events.get(n, ()):
+            event()
+
     for i in (0, 1):
         far_pass(4, i)
-    for slot in (1, 2, 3):
-        arrival(returned.at[(group + 4 - slot) % 4], ret_recv.at[slot - 1])
     twin_arrivals(near, co_recv)
 
-    def project_out(columns):
+    def side_of(which, begin, width):
+        return pl.ds(pl.multiple_of(SHARED + which * FAR + begin, 256), width)
+
+    columns = (
+        (((near, 0, 512),), ((0, pl.ds(0, 512)),)),
+        (((near, SHARED, 512),), ((0, side_of(side, 0, 512)),)),
+        (((far, 0, 512),), ((0, side_of(1 - side, 0, 512)),)),
+        (
+            ((near, SHARED + 512, 256), (far, 512, 256)),
+            ((0, side_of(side, 512, 256)), (256, side_of(1 - side, 512, 256))),
+        ),
+    )
+
+    def project_out(groups, lies):
         total = None
-        for g in range(4):
+        for g in groups:
             w = [
-                buf[g * 4 : (g + 1) * 4, :, begin : begin + width].reshape(512, width)
-                for buf, begin, width in columns
+                buf[span(g, 4), :, begin : begin + width].reshape(512, width)
+                for buf, begin, width in lies
             ]
             w = w[0] if len(w) == 1 else jnp.concatenate(w, axis=1)
             d = jnp.dot(returned[g], w, preferred_element_type=F32)
             total = d if total is None else total + d
-        return total, jnp.sum(total * total, axis=-1, keepdims=True)
-
-    def side_of(which, begin, width):
-        return pl.ds(pl.multiple_of(SHARED + which * FAR + begin, 256), width)
-
-    total, squares = project_out([(near, 0, 512)])
-    projected[:, 0:SHARED] = total
-    total, more = project_out([(near, SHARED, 512)])
-    projected[:, side_of(side, 0, 512)] = total
-    squares = squares + more
-    twin_arrivals(far, cf_recv)
-    total, more = project_out([(far, 0, 512)])
-    projected[:, side_of(1 - side, 0, 512)] = total
-    squares = squares + more
-    total, more = project_out([(near, SHARED + 512, 256), (far, 512, 256)])
-    projected[:, side_of(side, 512, 256)] = total[:, 0:256]
-    projected[:, side_of(1 - side, 512, 256)] = total[:, 256:512]
-    squares = squares + more
+        return total
+
+    def returns(slot):
+        source = (group + 4 - slot) % 4
+        for part in (0, 1):
+            two = pl.ds(part * 2 * HEAD, 2 * HEAD)
+            arrival(returned.at[source, :, two], ret_recv.at[slot - 1, part])
+
+    returns(2)
+    for n, (lies, places) in enumerate(columns):
+        if n == 2:
+            twin_arrivals(far, cf_recv)
+        total = project_out((group, (group + 2) % 4), lies)
+        for begin, place in places:
+            projected[:, place] = total[:, begin : begin + place.size]
+    returns(1)
+    returns(3)
+    squares = jnp.zeros((ROWS, 1), F32)
+    for lies, places in columns:
+        total = project_out(((group + 3) % 4, (group + 1) % 4), lies)
+        for begin, place in places:
+            value = projected[:, place] + total[:, begin : begin + place.size]
+            projected[:, place] = value
+            squares = squares + jnp.sum(value * value, axis=-1, keepdims=True)
     scale = lax.rsqrt(squares * (1.0 / WIDTH) + EPS)
-    out[0] = (projected[...] * scale * out_gain[...]).astype(BF16)
+    written = []
+    for n in range(4):
+        rows = slice(n * (ROWS // 4), (n + 1) * (ROWS // 4))
+        mixed[rows, :] = (projected[rows, :] * scale[rows] * out_gain[...]).astype(BF16)
+        written.append(
+            pltpu.make_async_copy(mixed.at[pl.ds(n * (ROWS // 4), ROWS // 4)], out.at[0, pl.ds(n * (ROWS // 4), ROWS // 4)], out_sem.at[n])
+        )
+        written[-1].start()
 
     for copy in sent:
         copy.wait_send()
+    for copy in written:
+        copy.wait()
 
 
 def on_device(tokens, in_gain, wq, wk, wv, q_gain, k_gain, wo, out_gain):
-    vmem = pl.BlockSpec(memory_space=pltpu.VMEM)
     hbm = pl.BlockSpec(memory_space=pl.ANY)
     dma = pltpu.SemaphoreType.DMA
     ring, other_core = dma((2, 4, 2)), dma((Z, 2))
@@ -619,7 +643,7 @@
         kernel,
         out_shape=jax.ShapeDtypeStruct((1, ROWS, WIDTH), BF16),
         in_specs=[hbm] * 9,
-        out_specs=vmem,
+        out_specs=hbm,
         scratch_shapes=[
             pltpu.VMEM((1, WIDTH), F32),
             pltpu.VMEM((1, HEAD), F32),
@@ -652,15 +676,17 @@
             pltpu.VMEM((GROUP, ROWS, 512), BF16),
             pltpu.VMEM((GROUP, ROWS, 512), BF16),
             pltpu.VMEM((ROWS, WIDTH), F32),
+            pltpu.VMEM((ROWS, WIDTH), BF16),
             dma((9,)),
+            dma((4,)),
             dma((6,)),
             dma((6,)),
             *([ring, ring, other_core, other_core] * 3),
             *([other_core] * 4),
             dma((12,)),
             dma((12,)),
-            dma((3,)),
-            dma((3,)),
+            dma((3, 2)),
+            dma((3, 2)),
         ],
         compiler_params=pltpu.CompilerParams(
             collective_id=0, has_side_effects=True, vmem_limit_bytes=60 * 2**20

time: 75.9 us -> 73.1 us (0.963)
  the two profiles are of different devices: /device:TPU:22 before, /device:TPU:1 now
where the time goes in v4:
time: 73.1 us; the launch traced here: 73 us
  Pallas kernels  70.7 us (97%)
  local copies, waits for them, and re-layouts  2.3 us (3%)
    pallas_call x1, Pallas kernels, on_device(): pl.pallas_call(kernel, out_shape=jax.ShapeDtypeStruct((1, ROWS, WIDTH), B...  70.7 us
    unnamed x1, local copies, waits for them, and re-layouts  2.3 us

profile of v4, /device:TPU:1, one launch (start us, length us, event | category | flops | bytes accessed | tf_op | source)
XLA Modules:
  0.0 73.0 jit_solution(7196103845867262959)
XLA Ops:
  0.0 70.7 %grouped_attention.1 = bf16[1,256,2048]{2,1,0:T(8,128)(2,1)} custom-call(bf16[1,256,2048]{2,1,0:T(8,128)(2,1)} %tokens_in.1, f32[1,2048]{1,0:T(1,128)} %bitcast.4, bf16[128,2048]{1,0:T(8,128)(2,1)} %wq_in.1, bf16[128,512]{1,0:T(8,128)(2,1)} %wk_in.1, bf16[128,512]{1,0:T(8,128)(2,1)} %wv_in.1, f32[1,128]{1,0:T(1,128)} %bitcast.6, f32[1,128]{1,0:T(1,128)} %bitcast.7, ...), custom_call_target="tpu_custom_call" | custom-call | tf_op jit(solution)/shard_map/grouped_attention/pallas_call | solution.py:642
  70.7 2.3 %copy.11 = bf16[1,256,2048]{2,1,0:T(8,128)(2,1)} copy(bf16[1,256,2048]{2,1,0:T(8,128)(2,1)} %grouped_attention.1) | data formatting | bytes 2097152

commit v5 on v4

--- a/solution.py
+++ b/solution.py
@@ -146,8 +146,6 @@
         copy.wait()
     pl.semaphore_wait(barrier, len(peers))
 
-    sent = []
-
     def send(src, dst, send_sem, recv_sem, to):
         copy = pltpu.make_async_remote_copy(
             src_ref=src,
@@ -158,21 +156,6 @@
             device_id_type=MESH,
         )
         copy.start()
-        return copy
-
-    def send_parts(pairs, whole, send_sem, recv_sem, to):
-        for src, dst in pairs:
-            send(src, dst, send_sem, recv_sem, to)
-        sent.append(
-            pltpu.make_async_remote_copy(
-                src_ref=whole,
-                dst_ref=whole,
-                send_sem=send_sem,
-                recv_sem=recv_sem,
-                device_id=to,
-                device_id_type=MESH,
-            )
-        )
 
     def arrival(ref, sem):
         pltpu.make_async_copy(ref, ref, sem).wait()
@@ -181,9 +164,7 @@
     nxt, prv = {"sp": member(1)}, {"sp": member(3)}
 
     def token_send(src, slot, part, index, to):
-        sent.append(
-            send(src, raw.at[slot - 1, part], ag_send.at[index], ag_recv.at[index], to)
-        )
+        send(src, raw.at[slot - 1, part], ag_send, ag_recv.at[index], to)
 
     token_send(tokens.at[low], 3, low, 0, nxt)
     token_send(tokens.at[high], 1, high, 1, prv)
@@ -198,33 +179,33 @@
 
     def kv_parts(i):
         mine = kv_weights.at[dp, chunks[i]]
-        pairs = [
+        return [
             (wk.at[chunks[i], kv_cols], mine.at[:, pl.ds(0, HEAD)]),
             (wv.at[chunks[i], kv_cols], mine.at[:, pl.ds(HEAD, HEAD)]),
         ]
-        return pairs, mine
 
     def q_parts(i):
         mine = q_weights.at[dp, chunks[i]]
-        return [(wq.at[chunks[i], q_cols], mine)], mine
+        return [(wq.at[chunks[i], q_cols], mine)]
 
     def near_parts(i):
         mine = near.at[dp, chunks[i]]
-        pairs = [
+        return [
             (wo.at[chunks[i], pl.ds(0, SHARED)], mine.at[:, pl.ds(0, SHARED)]),
             (wo.at[chunks[i], side_cols], mine.at[:, pl.ds(SHARED, FAR)]),
         ]
-        return pairs, mine
 
     def ring_start(parts, zs, zr):
         for turn in (0, 1):
             for way, to in ((0, up), (1, down)):
                 i = turn ^ way
-                send_parts(*parts(i), zs.at[way, 0, i], zr.at[way, 0, i], to)
+                for src, dst in parts(i):
+                    send(src, dst, zs, zr.at[way, 0, i], to)
 
     def twin_start(parts, cs, cr):
         for i in (0, 1):
-            send_parts(*parts(i), cs.at[0, i], cr.at[0, i], twin)
+            for src, dst in parts(i):
+                send(src, dst, cs, cr, twin)
 
     def source_of(way, step):
         return (((z + Z - step) % Z) if way == 0 else ((z + step) % Z)) * 2 + core
@@ -236,11 +217,8 @@
         part = buf.at[source_of(way, step), chunks[i]]
         arrival(part, zr.at[way, step - 1, i])
         if step < 3 or (step == 3 and i == way):
-            sent.append(
-                send(part, part, zs.at[way, step, i], zr.at[way, step, i], (up, down)[way])
-            )
-        slot = slot_of(way, step)
-        sent.append(send(part, part, cs.at[slot, i], cr.at[slot, i], twin))
+            send(part, part, zs, zr.at[way, step, i], (up, down)[way])
+        send(part, part, cs, cr, twin)
 
     def ring_events(ring, step, turns=(0, 1)):
         for turn in turns:
@@ -248,11 +226,8 @@
                 if step < 4 or turn == 0:
                     ring_event(*ring, way, step, turn ^ way)
 
-    def twin_arrivals(buf, cr, first=0):
-        for slot in range(first, Z):
-            source = ((z + Z - slot) % Z) * 2 + 1 - core
-            for i in (0, 1):
-                arrival(buf.at[source, chunks[i]], cr.at[slot, i])
+    def twin_arrivals(buf, cr):
+        arrival(buf.at[pl.ds(0, Z)], cr)
 
     kv_ring = (kv_weights, zk_send, zk_recv, ck_send, ck_recv)
     q_ring = (q_weights, zq_send, zq_recv, cq_send, cq_recv)
@@ -282,7 +257,7 @@
             normed[slot, part, :] = (v * lax.rsqrt(ms + EPS) * gain_in).astype(BF16)
             return c
 
-        lax.fori_loop(0, ROWS // 32, rows, 0)
+        lax.fori_loop(0, ROWS // 32, rows, 0, unroll=2)
 
     def angles(slot, c):
         row = lax.broadcasted_iota(jnp.int32, (ROWS, HEAD), 0)
@@ -348,14 +323,12 @@
 
     def kv_send_to(src, slot, what, half, to):
         index = kv_index(slot, what, half)
-        sent.append(
-            send(
-                kv_part(src, what, half),
-                kv_part(slot, what, half),
-                kv_send.at[index],
-                kv_recv.at[index],
-                {"sp": diagonal(to)},
-            )
+        send(
+            kv_part(src, what, half),
+            kv_part(slot, what, half),
+            kv_send.at[what],
+            kv_recv.at[index],
+            {"sp": diagonal(to)},
         )
 
     def kv_arrival(slot, what, half):
@@ -385,14 +358,11 @@
     twin_arrivals(q_weights, cq_recv)
     twin_start(near_parts, co_send, co_recv)
     for i in (0, 1):
-        part = far.at[dp, chunks[i]]
-        sent.append(
-            send(wo.at[chunks[i], other_cols], part, cf_send.at[0, i], cf_recv.at[0, i], twin)
-        )
+        send(wo.at[chunks[i], other_cols], far.at[dp, chunks[i]], cf_send, cf_recv, twin)
 
     gain_rows = jnp.broadcast_to(gain_q, (HEAD, HEAD)).T[:, 0:1]
 
-    def project_q(slot, c):
+    def project_q(slot):
         cut = q_weights[...].reshape(WIDTH, 512)
         values = jnp.dot(normed[slot], cut, preferred_element_type=F32)
         for h in range(4):
@@ -404,28 +374,27 @@
             q = q.astype(BF16).astype(F32) * (HEAD**-0.5 * LOG2E)
             coarse = q.astype(BF16)
             fine = (q - coarse.astype(F32)).astype(BF16)
-            cols = pl.ds(pl.multiple_of(slot * KEYS + h * ROWS, ROWS), ROWS)
+            cols = pl.ds(slot * KEYS + h * ROWS, ROWS)
             qt[0:HEAD, cols] = coarse
             qt[HEAD : 2 * HEAD, cols] = fine
-        return c
-
-    lax.fori_loop(0, 2, project_q, 0)
+
+    project_q(0)
+    project_q(1)
     ring_events(near_ring, 1, (0,))
-    lax.fori_loop(2, GROUP, project_q, 0)
+    project_q(2)
+    project_q(3)
     ring_events(near_ring, 1, (1,))
 
     def far_out(step, i):
         for way in (0, 1):
             if step < 4 or i == way:
                 source, slot = source_of(way, step), slot_of(way, step)
-                sent.append(
-                    send(
-                        near.at[source, chunks[i], pl.ds(SHARED, FAR)],
-                        far.at[source, chunks[i]],
-                        far_send.at[slot, i],
-                        far_recv.at[slot, i],
-                        (nxt, prv)[i],
-                    )
+                send(
+                    near.at[source, chunks[i], pl.ds(SHARED, FAR)],
+                    far.at[source, chunks[i]],
+                    far_send,
+                    far_recv.at[slot, i],
+                    (nxt, prv)[i],
                 )
 
     def far_pass(step, i):
@@ -434,7 +403,7 @@
                 slot = slot_of(way, step)
                 part = far.at[source_of(way, step), chunks[i]]
                 arrival(part, far_recv.at[slot, i])
-                sent.append(send(part, part, cf_send.at[slot, i], cf_recv.at[slot, i], twin))
+                send(part, part, cf_send, cf_recv, twin)
 
     ones = jnp.ones((ONES, KEYS), BF16)
     for d in range(GROUP):
@@ -485,14 +454,12 @@
             begin = (part * 2 + h) * HEAD
             attended[slot, :, begin : begin + HEAD] = scaled.T.astype(BF16)
         if slot:
-            sent.append(
-                send(
-                    attended.at[slot, :, two],
-                    returned.at[group, :, two],
-                    ret_send.at[slot - 1, part],
-                    ret_recv.at[slot - 1, part],
-                    {"sp": member(slot)},
-                )
+            send(
+                attended.at[slot, :, two],
+                returned.at[group, :, two],
+                ret_send,
+                ret_recv.at[slot - 1, part],
+                {"sp": member(slot)},
             )
         else:
             returned[group, :, two] = attended[0, :, two]
@@ -544,14 +511,14 @@
         far_pass(3, 1)
 
     events = {
-        3: [lambda: near_event(2, (0,))],
+        4: [lambda: near_event(2, (0,))],
         6: [keys_first],
         10: [lambda: near_event(2, (1,))],
         13: [lambda: near_event(3, (0,))],
         14: [keys_second],
         19: [lambda: near_event(3, (1,))],
         22: [keys_opposite],
-        25: [lambda: near_event(4, (0,))],
+        24: [lambda: near_event(4, (0,))],
         28: [far_third],
     }
 
@@ -629,8 +596,16 @@
         )
         written[-1].start()
 
-    for copy in sent:
-        copy.wait_send()
+    ring_bytes, twin_bytes = pl.ds(0, Z - 1), pl.ds(0, Z)
+    for buf, zs, _, cs, _ in (kv_ring, q_ring, near_ring):
+        arrival(buf.at[ring_bytes], zs)
+        arrival(buf.at[twin_bytes], cs)
+    arrival(far.at[ring_bytes], far_send)
+    arrival(far.at[twin_bytes], cf_send)
+    arrival(raw, ag_send)
+    arrival(kbuf.at[pl.ds(0, 3)], kv_send.at[0])
+    arrival(vbuf.at[pl.ds(0, 3), pl.ds(0, HEAD)], kv_send.at[1])
+    arrival(attended.at[pl.ds(0, 3)], ret_send)
     for copy in written:
         copy.wait()
 
@@ -638,7 +613,8 @@
 def on_device(tokens, in_gain, wq, wk, wv, q_gain, k_gain, wo, out_gain):
     hbm = pl.BlockSpec(memory_space=pl.ANY)
     dma = pltpu.SemaphoreType.DMA
-    ring, other_core = dma((2, 4, 2)), dma((Z, 2))
+    one = dma(())
+    ring = dma((2, 4, 2))
     return pl.pallas_call(
         kernel,
         out_shape=jax.ShapeDtypeStruct((1, ROWS, WIDTH), BF16),
@@ -679,13 +655,16 @@
             pltpu.VMEM((ROWS, WIDTH), BF16),
             dma((9,)),
             dma((4,)),
+            one,
             dma((6,)),
-            dma((6,)),
-            *([ring, ring, other_core, other_core] * 3),
-            *([other_core] * 4),
+            *([one, ring, one, one] * 3),
+            one,
+            dma((Z, 2)),
+            one,
+            one,
+            dma((2,)),
             dma((12,)),
-            dma((12,)),
-            dma((3, 2)),
+            one,
             dma((3, 2)),
         ],
         compiler_params=pltpu.CompilerParams(

time: 73.1 us -> 69.6 us (0.952)
  Pallas kernels: 70.7 us -> 66.8 us
    pallas_call x1, Pallas kernels: 70.7 us -> 66.8 us  [on_device(): pl.pallas_call(kernel, out_shape=jax.ShapeDtypeStruct((1, ROWS, WIDTH), B...]
where the time goes in v5:
time: 69.6 us; the launch traced here: 69.1 us
  Pallas kernels  66.8 us (96%)
  local copies, waits for them, and re-layouts  2.3 us (3%)
    pallas_call x1, Pallas kernels, on_device(): pl.pallas_call(kernel, out_shape=jax.ShapeDtypeStruct((1, ROWS, WIDTH), B...  66.8 us
    unnamed x1, local copies, waits for them, and re-layouts  2.3 us

profile of v5, /device:TPU:1, one launch (start us, length us, event | category | flops | bytes accessed | tf_op | source)
XLA Modules:
  0.0 69.1 jit_solution(15159912335491210935)
XLA Ops:
  0.0 66.8 %grouped_attention.1 = bf16[1,256,2048]{2,1,0:T(8,128)(2,1)} custom-call(bf16[1,256,2048]{2,1,0:T(8,128)(2,1)} %tokens_in.1, f32[1,2048]{1,0:T(1,128)} %bitcast.4, bf16[128,2048]{1,0:T(8,128)(2,1)} %wq_in.1, bf16[128,512]{1,0:T(8,128)(2,1)} %wk_in.1, bf16[128,512]{1,0:T(8,128)(2,1)} %wv_in.1, f32[1,128]{1,0:T(1,128)} %bitcast.6, f32[1,128]{1,0:T(1,128)} %bitcast.7, ...), custom_call_target="tpu_custom_call" | custom-call | tf_op jit(solution)/shard_map/grouped_attention/pallas_call | solution.py:618
  66.8 2.3 %copy.11 = bf16[1,256,2048]{2,1,0:T(8,128)(2,1)} copy(bf16[1,256,2048]{2,1,0:T(8,128)(2,1)} %grouped_attention.1) | data formatting | bytes 2097152

commit v6 on v5

--- a/solution.py
+++ b/solution.py
@@ -277,15 +277,17 @@
         return c
 
     normalize(tokens, 0)
+    lax.fori_loop(0, 2, angles, 0)
     ring_events(kv_ring, 1)
+    lax.fori_loop(2, 3, angles, 0)
     ring_events(q_ring, 1)
     ring_events(kv_ring, 2)
     arrival(raw.at[2, low], ag_recv.at[0])
     token_send(raw.at[2, low], 2, low, 4, nxt)
     arrival(raw.at[0, high], ag_recv.at[1])
     token_send(raw.at[0, high], 2, high, 5, prv)
+    lax.fori_loop(3, GROUP, angles, 0)
     ring_events(q_ring, 2)
-    lax.fori_loop(0, GROUP, angles, 0)
     ring_events(kv_ring, 3)
     ring_events(q_ring, 3)
     arrival(raw.at[2, high], ag_recv.at[2])
@@ -380,8 +382,8 @@
 
     project_q(0)
     project_q(1)
+    project_q(2)
     ring_events(near_ring, 1, (0,))
-    project_q(2)
     project_q(3)
     ring_events(near_ring, 1, (1,))
 
@@ -511,11 +513,10 @@
         far_pass(3, 1)
 
     events = {
-        4: [lambda: near_event(2, (0,))],
+        5: [lambda: near_event(2, (0,))],
         6: [keys_first],
         10: [lambda: near_event(2, (1,))],
-        13: [lambda: near_event(3, (0,))],
-        14: [keys_second],
+        14: [keys_second, lambda: near_event(3, (0,))],
         19: [lambda: near_event(3, (1,))],
         22: [keys_opposite],
         24: [lambda: near_event(4, (0,))],

time: 69.6 us -> 77.9 us (1.12)
  the two profiles are of different devices: /device:TPU:1 before, /device:TPU:2 now
where the time goes in v6:
time: 77.9 us; the launch traced here: 77.8 us
  Pallas kernels  75.5 us (97%)
  local copies, waits for them, and re-layouts  2.3 us (3%)
    pallas_call x1, Pallas kernels, on_device(): pl.pallas_call(kernel, out_shape=jax.ShapeDtypeStruct((1, ROWS, WIDTH), B...  75.5 us
    unnamed x1, local copies, waits for them, and re-layouts  2.3 us

profile of v6, /device:TPU:2, one launch (start us, length us, event | category | flops | bytes accessed | tf_op | source)
XLA Modules:
  0.0 77.8 jit_solution(5817451646360900735)
XLA Ops:
  0.0 75.5 %grouped_attention.1 = bf16[1,256,2048]{2,1,0:T(8,128)(2,1)} custom-call(bf16[1,256,2048]{2,1,0:T(8,128)(2,1)} %tokens_in.1, f32[1,2048]{1,0:T(1,128)} %bitcast.4, bf16[128,2048]{1,0:T(8,128)(2,1)} %wq_in.1, bf16[128,512]{1,0:T(8,128)(2,1)} %wk_in.1, bf16[128,512]{1,0:T(8,128)(2,1)} %wv_in.1, f32[1,128]{1,0:T(1,128)} %bitcast.6, f32[1,128]{1,0:T(1,128)} %bitcast.7, ...), custom_call_target="tpu_custom_call" | custom-call | tf_op jit(solution)/shard_map/grouped_attention/pallas_call | solution.py:619
  75.5 2.3 %copy.11 = bf16[1,256,2048]{2,1,0:T(8,128)(2,1)} copy(bf16[1,256,2048]{2,1,0:T(8,128)(2,1)} %grouped_attention.1) | data formatting | bytes 2097152
